TPU v7x, 256 devices: a whole 4x4x8 slice. The times are simulated.
256 devices in a mesh: ep: 16 (over y, x), tp: 16 (over z, core).
Axes of the slice: x: 4, y: 4, z: 8, core: 2. Of those that a mesh axis runs over, the one named last changes fastest.
Arguments:
- queries: bfloat16 [16384, 1024], P('ep', 'tp'), may hold values from -30 to 30
- key_vectors: bfloat16 [16384, 1024], P('ep', 'tp'), may hold values from -30 to 30
- value_vectors: bfloat16 [16384, 1024], P('ep', 'tp'), may hold values from -9 to 9
- cumulative_gate: float32 [16384, 16], P('ep', 'tp'), as said below
- out_weight: bfloat16 [1024, 2048], P('tp'), may hold values from -0.1875 to 0.1875
- expert_tokens: bfloat16 [24576, 2048], P(('ep', 'tp')), may hold values from -6 to 6
- norm_gain: float32 [2048], replicated, may hold values from 0.1 to 1.9
- gate_weight: bfloat16 [16, 2048, 2048], P('ep', None, 'tp'), may hold values from -0.375 to 0.375
- up_weight: bfloat16 [16, 2048, 2048], P('ep', None, 'tp'), may hold values from -0.375 to 0.375
- down_weight: bfloat16 [16, 2048, 2048], P('ep', 'tp'), may hold values from -0.015625 to 0.015625
- expert_choice: int32 [24576, 2], P(('ep', 'tp')), may hold values from 0 to 15, all different within a row; in each aligned block of 96 rows (0 to 95, 96 to 191, ...) at most 13 rows name the same one
- route_weights: float32 [24576, 2], P(('ep', 'tp')), may hold values from 0.2 to 1
Outputs:
- mixer_output: bfloat16 [16384, 2048], P(('ep', 'tp'))
- expert_output: bfloat16 [24576, 2048], P(('ep', 'tp'))
Inputs may be any that keep to these rules, and one draw needn't show every extreme that they name: `cumulative_gate`: each head's values never rise from one position to the next. `expert_choice`: each row names 2 different experts; within the rows of one device no expert is named more than 13 times, and in some of them one expert exactly 13 times.
All inputs are finite; a program needn't handle non-finite values.
Results may differ from a plain program's by a relative error of at most 0.019.
Values may be sent and summed in bfloat16 or wider, within the bound.
A program may use at most 128 MiB of HBM per device.

v0:
```python
import functools
import math

import jax
import jax.numpy as jnp
from jax import lax
from jax.experimental import pallas as pl
from jax.experimental.pallas import tpu as pltpu
from jax.sharding import PartitionSpec as P

EXPERTS = 16
CAP = 13
SLOT = 16
TQ = 256

eps_norm = 1e-05
clamp_limit = 7.0
sig_alpha = 1.702
floor_score = -1e30


def attend_block(q_ref, cq_ref, kv, ck_row, m_ref, l_ref, acc_ref, diagonal):
    width = kv.shape[0]

    def one_tile(i, carry):
        rows = pl.ds(pl.multiple_of(i * TQ, TQ), TQ)
        s = lax.dot_general(
            q_ref[rows, :], kv, (((1,), (1,)), ((), ())), preferred_element_type=jnp.float32
        )
        s = s + (cq_ref[rows, :] - ck_row)
        if diagonal:
            q_pos = i * TQ + lax.broadcasted_iota(jnp.int32, (TQ, width), 0)
            k_pos = lax.broadcasted_iota(jnp.int32, (TQ, width), 1)
            s = jnp.where(k_pos <= q_pos, s, floor_score)
        top = jnp.max(s, axis=1, keepdims=True)
        if diagonal:
            p = jnp.exp(s - top)
            m_ref[rows, :] = jnp.broadcast_to(top, (TQ, 128))
            l_ref[rows, :] = jnp.broadcast_to(jnp.sum(p, axis=1, keepdims=True), (TQ, 128))
            acc_ref[rows, :] = jnp.dot(
                p.astype(jnp.bfloat16), kv, preferred_element_type=jnp.float32
            )
        else:
            old = m_ref[rows, :]
            new = jnp.maximum(old, top)
            shrink = jnp.exp(old - new)
            p = jnp.exp(s - new[:, :1])
            m_ref[rows, :] = new
            l_ref[rows, :] = l_ref[rows, :] * shrink + jnp.sum(p, axis=1, keepdims=True)
            acc_ref[rows, :] = acc_ref[rows, :] * shrink + jnp.dot(
                p.astype(jnp.bfloat16), kv, preferred_element_type=jnp.float32
            )
        return carry

    lax.fori_loop(0, q_ref.shape[0] // TQ, one_tile, 0)


def gate_row(tile):
    return jnp.concatenate([tile[r : r + 1, :] for r in range(tile.shape[0])], axis=1)


def attention_kernel(q_ref, cq_ref, kv_ref, ck_ref, out_ref, m_ref, l_ref, acc_ref):
    me = lax.axis_index("ep")
    attend_block(q_ref, cq_ref, kv_ref[me], gate_row(ck_ref[me]), m_ref, l_ref, acc_ref, True)

    def step(k, carry):
        j = me - k
        attend_block(q_ref, cq_ref, kv_ref[j], gate_row(ck_ref[j]), m_ref, l_ref, acc_ref, False)
        return carry

    lax.fori_loop(1, me + 1, step, 0)
    out_ref[...] = (acc_ref[...] / l_ref[...])[:, 64:].astype(jnp.bfloat16)


def activate(g, u):
    g = jnp.minimum(g, clamp_limit)
    u = jnp.clip(u, -clamp_limit, clamp_limit)
    return (g * jax.nn.sigmoid(sig_alpha * g) * (u + 1.0)).astype(jnp.bfloat16)


def expert_kernel(x_ref, g_ref, u_ref, d_ref, out_ref, acc_ref):
    step = pl.program_id(0)
    x = x_ref[...]
    g = jnp.dot(x, g_ref[...], preferred_element_type=jnp.float32)
    u = jnp.dot(x, u_ref[...], preferred_element_type=jnp.float32)
    part = jnp.dot(activate(g, u), d_ref[...], preferred_element_type=jnp.float32)

    @pl.when(step == 0)
    def _():
        acc_ref[...] = part

    @pl.when(step > 0)
    def _():
        acc_ref[...] += part

    @pl.when(step == pl.num_programs(0) - 1)
    def _():
        out_ref[...] = acc_ref[...].astype(jnp.bfloat16)


def route(expert_choice, route_weights):
    flat_ids = expert_choice.reshape(-1)
    one_hot = (flat_ids[:, None] == jnp.arange(EXPERTS, dtype=jnp.int32)[None, :]).astype(jnp.int32)
    slot_rank = jnp.sum((jnp.cumsum(one_hot, axis=0) - one_hot) * one_hot, axis=1)
    slot_ids = (flat_ids * SLOT + slot_rank).reshape(expert_choice.shape)
    table = slot_ids[:, :, None] == jnp.arange(EXPERTS * SLOT, dtype=jnp.int32)[None, None, :]
    placing = jnp.sum(table.astype(jnp.bfloat16), axis=1)
    combine = jnp.sum(jnp.where(table, route_weights[:, :, None], 0.0), axis=1)
    return placing, combine


def local(
    queries,
    key_vectors,
    value_vectors,
    cumulative_gate,
    out_weight,
    expert_tokens,
    norm_gain,
    gate_weight,
    up_weight,
    down_weight,
    expert_choice,
    route_weights,
):
    width = expert_tokens.shape[1]
    block_rows = queries.shape[0]
    n_ep = lax.axis_size("ep")
    n_tp = lax.axis_size("tp")
    kv = jnp.concatenate([key_vectors, value_vectors], axis=1)
    kv_all = lax.all_gather(kv, "ep", axis=0, tiled=True).reshape(n_ep, block_rows, 128)
    gate_tile = cumulative_gate.reshape(block_rows // 128, 128)
    gates_all = lax.all_gather(gate_tile, "ep", axis=0)
    gate_all = lax.all_gather(gate_weight[0], "tp", axis=0, tiled=True)
    up_all = lax.all_gather(up_weight[0], "tp", axis=0, tiled=True)
    down_all = lax.all_gather(down_weight[0], "tp", axis=0, tiled=True)
    out_all = lax.all_gather(out_weight, "tp", axis=0, tiled=True)

    tokens_float = expert_tokens.astype(jnp.float32)
    normed = (
        tokens_float
        * lax.rsqrt(jnp.mean(tokens_float * tokens_float, axis=1, keepdims=True) + eps_norm)
        * norm_gain
    ).astype(jnp.bfloat16)
    placing, combine = route(expert_choice, route_weights)
    outgoing = jnp.einsum("ts,td->sd", placing, normed, preferred_element_type=jnp.float32).astype(
        jnp.bfloat16
    )
    arrived = lax.all_to_all(
        outgoing.reshape(EXPERTS, SLOT, width), "ep", split_axis=0, concat_axis=0, tiled=True
    ).reshape(-1, width)

    head = queries.shape[1]
    q_wide = jnp.pad(queries * jnp.bfloat16(1.0 / math.sqrt(head)), ((0, 0), (0, 128 - head)))
    attention = pl.pallas_call(
        attention_kernel,
        out_shape=jax.ShapeDtypeStruct((block_rows, head), jnp.bfloat16),
        in_specs=[pl.BlockSpec(memory_space=pltpu.VMEM)] * 4,
        out_specs=pl.BlockSpec(memory_space=pltpu.VMEM),
        scratch_shapes=[pltpu.VMEM((block_rows, 128), jnp.float32)] * 3,
        compiler_params=pltpu.CompilerParams(vmem_limit_bytes=40 * 2**20),
        cost_estimate=pl.CostEstimate(flops=10**10, bytes_accessed=6 * 10**6, transcendentals=0),
        name="attend",
    )(q_wide, cumulative_gate, kv_all, gates_all)
    pieces = lax.all_to_all(
        attention.reshape(n_tp, block_rows // n_tp, head), "tp", split_axis=0, concat_axis=0
    )
    heads = pieces.transpose(1, 0, 2).reshape(block_rows // n_tp, n_tp * head)
    mixer_output = jnp.dot(heads, out_all, preferred_element_type=jnp.float32).astype(jnp.bfloat16)

    units = gate_weight.shape[2]
    rows = arrived.shape[0]
    results = pl.pallas_call(
        expert_kernel,
        grid=(n_tp,),
        out_shape=jax.ShapeDtypeStruct((rows, width), jnp.bfloat16),
        in_specs=[
            pl.BlockSpec((rows, width), lambda i: (0, 0)),
            pl.BlockSpec((width, units), lambda i: (i, 0)),
            pl.BlockSpec((width, units), lambda i: (i, 0)),
            pl.BlockSpec((units, width), lambda i: (i, 0)),
        ],
        out_specs=pl.BlockSpec((rows, width), lambda i: (0, 0)),
        scratch_shapes=[pltpu.VMEM((rows, width), jnp.float32)],
        compiler_params=pltpu.CompilerParams(vmem_limit_bytes=40 * 2**20),
        cost_estimate=pl.CostEstimate(flops=10**10, bytes_accessed=26 * 10**6, transcendentals=0),
        name="experts",
    )(arrived, gate_all, up_all, down_all)
    returned = lax.all_to_all(
        results.reshape(n_ep, SLOT, width), "ep", split_axis=0, concat_axis=0, tiled=True
    ).reshape(-1, width)
    expert_output = jnp.dot(
        combine, returned.astype(jnp.float32), precision=lax.Precision.HIGHEST
    ).astype(jnp.bfloat16)
    return (mixer_output, expert_output)


def solution(mesh):
    placed = (
        P("ep", "tp"),
        P("ep", "tp"),
        P("ep", "tp"),
        P("ep", "tp"),
        P("tp", None),
        P(("ep", "tp"), None),
        P(),
        P("ep", None, "tp"),
        P("ep", None, "tp"),
        P("ep", "tp", None),
        P(("ep", "tp"), None),
        P(("ep", "tp"), None),
    )
    return jax.shard_map(
        local,
        mesh=mesh,
        in_specs=placed,
        out_specs=(P(("ep", "tp"), None), P(("ep", "tp"), None)),
        check_vma=False,
    )
```

profile of v0, /device:TPU:1, one launch (start us, length us, event | category | flops | bytes accessed | tf_op | source)
XLA Modules:
  0.0 309.4 jit_solution(13148436434383710652)
XLA Ops:
  7.2 0.0 copy-start.2
  7.2 0.0 copy-start.3
  7.2 0.0 all-gather.9.cloned.1.call-start
  7.2 1.7 pad_maximum_fusion
  8.9 0.0 all-gather.9.cloned.1.call-update
  9.0 0.0 all-gather.13.cloned.1.call-start
  9.0 0.7 all-gather.13.cloned.1.call-update
  9.7 0.0 all-gather.15.cloned.1.call-start
  9.8 0.7 all-gather.15.cloned.1.call-update
  10.4 0.0 all-gather.17.cloned.1.call-start
  10.5 0.5 all-gather.17.cloned.1.call-update
  11.0 0.0 all-gather.11.cloned.1.call-start
  11.1 0.5 all-gather.11.cloned.1.call-update
  11.6 0.8 copy.54
  12.4 0.1 eq.35
  12.5 0.6 reduce-window.6
  13.1 0.2 slice_reduce_fusion
  13.4 0.1 bitcast_bitcast_fusion
  13.5 0.1 reduce_sum.42
  13.6 0.1 copy.57
  13.7 0.7 multiply_add_fusion
  14.4 0.1 fusion.7
  14.5 1.2 fusion
  15.7 2.5 convolution_convert_fusion
  18.2 7.6 %all-to-all-start.1 = ((bf16[16,16,2048]{2,1,0:T(8,128)(2,1)}), bf16[16,16,2048]{2,1,0:T(8,128)(2,1)S(1)}, u32[]{:S(2)}, u32[]{:S(2)}) async-start(bf16[16,16,2048]{2,1,0:T(8,128)(2,1)} %bitcast.5), calls=%async_computation.1 | async-start | bytes 2097152 | tf_op jit(solution)/shard_map/all_to_all | solution.py:149
  25.8 0.0 copy-done.2
  25.8 0.2 copy.49
  26.0 0.0 copy-done.3
  26.0 0.2 copy.52.cq_ref
  26.2 0.1 pad.8.q_ref
  26.3 29.5 %all_gather.19.ck_ref = f32[16,8,128]{2,1,0:T(8,128)S(1)} all-gather(f32[1,8,128]{2,1,0:T(8,128)S(1)} %bitcast.34), channel_id=1, replica_groups=mesh['ep'=16,'tp'=16] {'ep'}, dimensions={0}, use_global_device_ids=true | all-gather | bytes 69632 | tf_op jit(solution)/shard_map/all_gather | solution.py:133
  55.8 24.3 %all-gather.9.cloned.1.call-done = bf16[16384,128]{0,1:T(8,128)(2,1)} async-done(((bf16[1024,128]{0,1:T(8,128)(2,1)}), bf16[16384,128]{0,1:T(8,128)(2,1)}) %all-gather.9.cloned.1.call-update) | async-done | bytes 4194320 | tf_op jit(solution)/shard_map/all_gather | solution.py:131
  80.1 6.4 %copy.51 = bf16[16384,128]{1,0:T(8,128)(2,1)} copy(bf16[16384,128]{0,1:T(8,128)(2,1)} %all-gather.9.cloned.1.call-done) | data formatting | bytes 8388608 | tf_op jit(solution)/shard_map/all_gather | solution.py:131
  86.5 0.0 copy-start
  86.5 2.2 copy-done
  88.7 3.3 %attend.1 = bf16[1024,64]{1,0:T(8,128)(2,1)S(1)} custom-call(bf16[1024,128]{1,0:T(8,128)(2,1)S(1)} %pad.8.q_ref, f32[1024,1]{1,0:T(8,128)S(1)} %copy.52.cq_ref, bf16[16,1024,128]{2,1,0:T(8,128)(2,1)S(1)} %bitcast.28, f32[16,8,128]{2,1,0:T(8,128)S(1)} %all_gather.19.ck_ref), custom_call_target="tpu_custom_call" | custom-call | flops 10000000000 | bytes 6000000 | tf_op jit(solution)/shard_map/attend/pallas_call | solution.py:155
  91.9 0.9 reshape.68
  92.8 0.0 all-to-all-done.1
  92.8 7.9 %all-to-all-start = ((bf16[16,2,2048]{2,1,0:T(2,128)(2,1)}), bf16[16,2,2048]{2,1,0:T(2,128)(2,1)S(1)}, u32[]{:S(2)}, u32[]{:S(2)}) async-start(bf16[16,2,2048]{2,1,0:T(2,128)(2,1)} %reshape.68), calls=%async_computation | async-start | bytes 262144 | tf_op jit(solution)/shard_map/all_to_all | solution.py:165
  100.7 40.2 %all-gather.13.cloned.1.call-done = bf16[1,32768,128]{2,1,0:T(8,128)(2,1)} async-done(((bf16[1,2048,128]{2,1,0:T(8,128)(2,1)}), bf16[1,32768,128]{2,1,0:T(8,128)(2,1)}) %all-gather.13.cloned.1.call-update) | async-done | bytes 8388624 | tf_op jit(solution)/shard_map/all_gather | solution.py:134
  140.9 54.8 %all-gather.15.cloned.1.call-done = bf16[1,32768,128]{2,1,0:T(8,128)(2,1)} async-done(((bf16[1,2048,128]{2,1,0:T(8,128)(2,1)}), bf16[1,32768,128]{2,1,0:T(8,128)(2,1)}) %all-gather.15.cloned.1.call-update) | async-done | bytes 8388624 | tf_op jit(solution)/shard_map/all_gather | solution.py:135
  195.6 56.8 %all-gather.17.cloned.1.call-done = bf16[1,2048,2048]{2,1,0:T(8,128)(2,1)} async-done(((bf16[1,128,2048]{2,1,0:T(8,128)(2,1)}), bf16[1,2048,2048]{2,1,0:T(8,128)(2,1)}) %all-gather.17.cloned.1.call-update) | async-done | bytes 8388624 | tf_op jit(solution)/shard_map/all_gather | solution.py:136
  252.4 0.0 copy-start.1
  252.4 3.4 %copy-done.1 = bf16[1,32768,128]{2,1,0:T(8,128)(2,1)S(1)} copy-done((bf16[1,32768,128]{2,1,0:T(8,128)(2,1)S(1)}, bf16[1,32768,128]{2,1,0:T(8,128)(2,1)}, u32[]{:S(2)}) %copy-start.1) | copy-done | bytes 8388632
  255.8 0.0 copy-start.4
  255.8 22.6 %experts.1 = bf16[256,2048]{1,0:T(8,128)(2,1)} custom-call(bf16[256,2048]{1,0:T(8,128)(2,1)S(1)} %bitcast.29, bf16[32768,128]{1,0:T(8,128)(2,1)S(1)} %bitcast.31, bf16[32768,128]{1,0:T(8,128)(2,1)} %bitcast.35, bf16[2048,2048]{1,0:T(8,128)(2,1)} %bitcast.36), custom_call_target="tpu_custom_call" | custom-call | flops 10000000000 | bytes 26000000 | tf_op jit(solution)/shard_map/experts/pallas_call | solution.py:173
  278.4 0.0 all-to-all-done
  278.4 6.5 %all-to-all-start.2 = ((bf16[16,16,2048]{2,1,0:T(8,128)(2,1)}), bf16[16,16,2048]{2,1,0:T(8,128)(2,1)S(1)}, u32[]{:S(2)}, u32[]{:S(2)}) async-start(bf16[16,16,2048]{2,1,0:T(8,128)(2,1)} %bitcast.10), calls=%async_computation.2 | async-start | bytes 2097152 | tf_op jit(solution)/shard_map/all_to_all | solution.py:189
  285.0 0.0 copy-done.4
  285.0 0.1 select_reduce_fusion
  285.1 0.2 reshape.69
  285.3 0.2 copy.53
  285.5 0.2 reshape.56
  285.7 8.8 %all-gather.11.cloned.1.call-done = bf16[1024,2048]{1,0:T(8,128)(2,1)} async-done(((bf16[64,2048]{1,0:T(8,128)(2,1)}), bf16[1024,2048]{1,0:T(8,128)(2,1)}) %all-gather.11.cloned.1.call-update) | async-done | bytes 4194320 | tf_op jit(solution)/shard_map/all_gather | solution.py:137
  294.5 3.7 %convolution_convert_fusion.2 = bf16[64,2048]{1,0:T(8,128)(2,1)} fusion(bf16[64,1024]{1,0:T(8,128)(2,1)S(1)} %reshape.56, bf16[1024,2048]{1,0:T(8,128)(2,1)} %all-gather.11.cloned.1.call-done), kind=kOutput, calls=%fused_computation.2 | convolution fusion | flops 268566528 | bytes 4587520 | tf_op jit(solution)/shard_map/dot_general | solution.py:169
  298.3 3.2 %all-to-all-done.2 = bf16[16,16,2048]{2,1,0:T(8,128)(2,1)S(1)} async-done(((bf16[16,16,2048]{2,1,0:T(8,128)(2,1)}), bf16[16,16,2048]{2,1,0:T(8,128)(2,1)S(1)}, u32[]{:S(2)}, u32[]{:S(2)}) %all-to-all-start.2) | async-done | bytes 1048608 | tf_op jit(solution)/shard_map/all_to_all | solution.py:189
  301.5 1.4 convolution_convert_fusion.1
  (7 shorter events, 0.1 us)
Async XLA Ops:
  7.2 18.6 %copy-start.2 = (bf16[1024,64]{0,1:T(8,128)(2,1)S(1)}, bf16[1024,64]{0,1:T(8,128)(2,1)}, u32[]{:S(2)}) copy-start(bf16[1024,64]{0,1:T(8,128)(2,1)} %param.12) | copy-start | bytes 393220
  7.2 18.8 %copy-start.3 = (f32[1024,1]{0,1:T(1,128)S(1)}, f32[1024,1]{0,1:T(1,128)}, u32[]{:S(2)}) copy-start(f32[1024,1]{0,1:T(1,128)} %param.15) | copy-start | bytes 12292
  7.2 72.9 %all-gather.9.cloned.1.call-start = ((), (), s32[]{:S(2)}) async-start(), calls=%async_computation.3 | async-start | bytes 4456448 | tf_op jit(solution)/shard_map/all_gather | solution.py:131
  9.0 131.9 %all-gather.13.cloned.1.call-start = ((), (), s32[]{:S(2)}) async-start(), calls=%async_computation.5 | async-start | bytes 8912896 | tf_op jit(solution)/shard_map/all_gather | solution.py:134
  9.7 185.9 %all-gather.15.cloned.1.call-start = ((), (), s32[]{:S(2)}) async-start(), calls=%async_computation.6 | async-start | bytes 8912896 | tf_op jit(solution)/shard_map/all_gather | solution.py:135
  10.4 242.0 %all-gather.17.cloned.1.call-start = ((), (), s32[]{:S(2)}) async-start(), calls=%async_computation.7 | async-start | bytes 8912896 | tf_op jit(solution)/shard_map/all_gather | solution.py:136
  11.0 283.5 %all-gather.11.cloned.1.call-start = ((), (), s32[]{:S(2)}) async-start(), calls=%async_computation.4 | async-start | bytes 4456448 | tf_op jit(solution)/shard_map/all_gather | solution.py:137
  18.2 74.7 %all-to-all-start.1 = ((bf16[16,16,2048]{2,1,0:T(8,128)(2,1)}), bf16[16,16,2048]{2,1,0:T(8,128)(2,1)S(1)}, u32[]{:S(2)}, u32[]{:S(2)}) async-start(bf16[16,16,2048]{2,1,0:T(8,128)(2,1)} %bitcast.5), calls=%async_computation.1 | async-start | bytes 2097152 | tf_op jit(solution)/shard_map/all_to_all | solution.py:149
  86.5 2.2 copy-start
  92.8 185.6 %all-to-all-start = ((bf16[16,2,2048]{2,1,0:T(2,128)(2,1)}), bf16[16,2,2048]{2,1,0:T(2,128)(2,1)S(1)}, u32[]{:S(2)}, u32[]{:S(2)}) async-start(bf16[16,2,2048]{2,1,0:T(2,128)(2,1)} %reshape.68), calls=%async_computation | async-start | bytes 262144 | tf_op jit(solution)/shard_map/all_to_all | solution.py:165
  252.4 3.4 %copy-start.1 = (bf16[1,32768,128]{2,1,0:T(8,128)(2,1)S(1)}, bf16[1,32768,128]{2,1,0:T(8,128)(2,1)}, u32[]{:S(2)}) copy-start(bf16[1,32768,128]{2,1,0:T(8,128)(2,1)} %all-gather.13.cloned.1.call-done) | copy-start | bytes 25165828
  255.8 29.2 %copy-start.4 = (f32[96,2]{0,1:T(2,128)S(1)}, f32[96,2]{0,1:T(2,128)}, u32[]{:S(2)}) copy-start(f32[96,2]{0,1:T(2,128)} %param.23) | copy-start | bytes 2308
  278.4 23.0 %all-to-all-start.2 = ((bf16[16,16,2048]{2,1,0:T(8,128)(2,1)}), bf16[16,16,2048]{2,1,0:T(8,128)(2,1)S(1)}, u32[]{:S(2)}, u32[]{:S(2)}) async-start(bf16[16,16,2048]{2,1,0:T(8,128)(2,1)} %bitcast.10), calls=%async_computation.2 | async-start | bytes 2097152 | tf_op jit(solution)/shard_map/all_to_all | solution.py:189
Sparse Core Ops, SparseCore 0:
  11.0 69.0 all-gather.8
  81.9 58.9 all-gather.12
  142.7 52.8 all-gather.14
  197.3 55.0 all-gather.16
  254.1 40.3 all-gather.10
where the time goes:
time: 310 us; the launch traced here: 309 us
  waiting for transfers between devices  190 us (61%)
  blocking collectives  29.5 us (10%)
  Pallas kernels  25.9 us (8%)
  starting transfers between devices  22.2 us (7%)
  local copies, waits for them, and re-layouts  15.2 us (5%)
  between operations  13.9 us (4%)
  matrix products  7.61 us (2%)
  other arithmetic  4.56 us (1%)
    all_gather x1, waiting for transfers between devices, local(): down_all = lax.all_gather(down_weight[0], 'tp', axis=0, tiled=True)  56.8 us
    all_gather x1, waiting for transfers between devices, local(): up_all = lax.all_gather(up_weight[0], 'tp', axis=0, tiled=True)  54.8 us
    all_gather x1, waiting for transfers between devices, local(): gate_all = lax.all_gather(gate_weight[0], 'tp', axis=0, tiled=True)  40.2 us
    all_gather x1, blocking collectives, local(): gates_all = lax.all_gather(gate_tile, 'ep', axis=0)  29.5 us
    all_gather x1, waiting for transfers between devices, local(): lax.all_gather(kv, 'ep', axis=0, tiled=True).reshape(n_ep, block_rows, 128)  24.3 us
    pallas_call x1, Pallas kernels, local(): pl.pallas_call(expert_kernel, grid=(n_tp,), out_shape=jax.ShapeDtypeStruc...  22.6 us
    all_gather x1, waiting for transfers between devices, local(): out_all = lax.all_gather(out_weight, 'tp', axis=0, tiled=True)  8.81 us
    all_to_all x1, starting transfers between devices, local(): lax.all_to_all(attention.reshape(n_tp, block_rows // n_tp, head), 'tp', s...  7.86 us
  transfers between devices with their start and end apart: 8, of which 6 were waited for; matrix products, arithmetic and copies ran while one was open for 6% of the time, Pallas kernels for 8%

commit v1 on v0

v1 whole, which is shorter than its diff:
```python
import functools
import math

import jax
import jax.numpy as jnp
from jax import lax
from jax.experimental import pallas as pl
from jax.experimental.pallas import tpu as pltpu
from jax.sharding import PartitionSpec as P

SLOT = 16
TQ = 256
HEAD = 64
MESH = pl.DeviceIdType.MESH

eps_norm = 1e-05
clamp_limit = 7.0
sig_alpha = 1.702
floor_score = -1e30


def gate_row(tile):
    return jnp.concatenate([tile[r : r + 1, :] for r in range(tile.shape[0])], axis=1)


def activate(g, u):
    g = jnp.minimum(g, clamp_limit)
    u = jnp.clip(u, -clamp_limit, clamp_limit)
    return (g * jax.nn.sigmoid(sig_alpha * g) * (u + 1.0)).astype(jnp.bfloat16)


def attend_block(q_ref, cq_ref, kv_ref, ck_ref, m_ref, l_ref, acc_ref, diagonal):
    width = kv_ref.shape[0]
    tile = min(TQ, q_ref.shape[0])
    ck_row = gate_row(ck_ref[...])

    def one_tile(i, carry):
        rows = pl.ds(pl.multiple_of(i * tile, tile), tile)
        kv = kv_ref[...]
        s = lax.dot_general(
            q_ref[rows, :], kv, (((1,), (1,)), ((), ())), preferred_element_type=jnp.float32
        )
        s = s + (cq_ref[rows, :] - ck_row)
        if diagonal:
            q_pos = i * tile + lax.broadcasted_iota(jnp.int32, (tile, width), 0)
            k_pos = lax.broadcasted_iota(jnp.int32, (tile, width), 1)
            s = jnp.where(k_pos <= q_pos, s, floor_score)
        top = jnp.max(s, axis=1, keepdims=True)
        if diagonal:
            p = jnp.exp(s - top)
            m_ref[rows, :] = jnp.broadcast_to(top, (tile, 128))
            l_ref[rows, :] = jnp.broadcast_to(jnp.sum(p, axis=1, keepdims=True), (tile, 128))
            acc_ref[rows, :] = jnp.dot(
                p.astype(jnp.bfloat16), kv, preferred_element_type=jnp.float32
            )
        else:
            old = m_ref[rows, :]
            new = jnp.maximum(old, top)
            shrink = jnp.exp(old - new)
            p = jnp.exp(s - new[:, :1])
            m_ref[rows, :] = new
            l_ref[rows, :] = l_ref[rows, :] * shrink + jnp.sum(p, axis=1, keepdims=True)
            acc_ref[rows, :] = acc_ref[rows, :] * shrink + jnp.dot(
                p.astype(jnp.bfloat16), kv, preferred_element_type=jnp.float32
            )
        return carry

    lax.fori_loop(0, q_ref.shape[0] // tile, one_tile, 0)


def body(
    n_ep,
    n_tp,
    q_ref,
    cq_ref,
    kv_ref,
    ck_ref,
    wg_ref,
    wu_ref,
    wd_ref,
    ow_ref,
    og_ref,
    comb_ref,
    mix_ref,
    eo_ref,
    kv_all,
    ck_all,
    rg,
    ru,
    rd,
    lg,
    lu,
    ld,
    x,
    acc,
    p_send,
    p_recv,
    res,
    ret,
    osl,
    w_all,
    att_send,
    att_in,
    mix_acc,
    mp_send,
    mp_recv,
    m_ref,
    l_ref,
    att_acc,
    s_kv,
    r_kv,
    s_ck,
    r_ck,
    s_og,
    r_og,
    s_res,
    r_res,
    s_osl,
    r_osl,
    s_w,
    r_w,
    s_att,
    r_att,
    s_ring,
    r_ring,
    s_pt,
    r_pt,
):
    nz = n_tp // 2
    hops = nz // 2 - 1
    ep = lax.axis_index("ep")
    tp = lax.axis_index("tp")
    z = lax.div(tp, 2)
    core = lax.rem(tp, 2)
    right = lax.rem(tp + 2, n_tp)
    left = lax.rem(tp + n_tp - 2, n_tp)
    partner = tp + 1 - 2 * core
    width = wg_ref.shape[0]
    col = width // n_ep
    t_dev = mp_send.shape[0]
    half_units = ld.shape[0] // 2

    def ep_peer(d):
        return lax.rem(ep + d, n_ep)

    def z_peer(d):
        return lax.rem(z + d, nz)

    def ep_copy(src, dst, send, recv, peer):
        return pltpu.make_async_remote_copy(
            src_ref=src, dst_ref=dst, send_sem=send, recv_sem=recv,
            device_id={"ep": peer}, device_id_type=MESH,
        )

    def tp_copy(src, dst, send, recv, peer):
        return pltpu.make_async_remote_copy(
            src_ref=src, dst_ref=dst, send_sem=send, recv_sem=recv,
            device_id={"tp": peer}, device_id_type=MESH,
        )

    def kv_copy(slot, peer):
        return ep_copy(kv_ref, kv_all.at[slot], s_kv.at[peer], r_kv.at[slot], peer)

    def ck_copy(slot, peer):
        return ep_copy(ck_ref, ck_all.at[slot], s_ck.at[peer], r_ck.at[slot], peer)

    def og_copy(slot, peer):
        return ep_copy(og_ref.at[peer], x.at[0, slot], s_og.at[peer], r_og.at[slot], peer)

    def res_copy(slot, peer):
        return ep_copy(res.at[peer], ret.at[slot], s_res.at[peer], r_res.at[slot], peer)

    def w_copy(slot, peer):
        return ep_copy(osl, w_all.at[slot], s_w.at[peer], r_w.at[slot], peer)

    my_cols = pl.ds(pl.multiple_of(ep * col, col), col)

    def osl_copy(slot, pz):
        return tp_copy(
            ow_ref.at[:, my_cols], osl.at[slot], s_osl.at[pz], r_osl.at[slot], 2 * pz + core
        )

    def att_copy(slot, pz):
        return tp_copy(
            att_send.at[pz], att_in.at[slot], s_att.at[pz], r_att.at[slot], 2 * pz + core
        )

    def pt_copy(src, dst, n):
        return tp_copy(src, dst, s_pt.at[n], r_pt.at[n], partner)

    own = (wg_ref, wu_ref, wd_ref)
    slots = (rg, ru, rd)
    peers = (right, left)

    def first_copy(direction, a):
        return tp_copy(
            own[a], slots[a].at[direction, 0], s_ring.at[direction, 0, a],
            r_ring.at[direction, 0, a], peers[direction],
        )

    def ring_copy(direction, h, a):
        return tp_copy(
            slots[a].at[direction, h - 1], slots[a].at[direction, h],
            s_ring.at[direction, h, a], r_ring.at[direction, h, a], peers[direction],
        )

    def last_copy(direction, a):
        src = slots[a].at[direction, hops - 1]
        if a == 0:
            dst = lg
        elif a == 1:
            dst = lu
        else:
            part = pl.ds(direction * half_units, half_units)
            src, dst = src.at[part], ld.at[part]
        return tp_copy(
            src, dst, s_ring.at[direction, hops, a], r_ring.at[direction, hops, a],
            peers[direction],
        )

    last_parts = ((0, 0), (1, 1), (0, 2), (1, 2))

    barrier = pltpu.get_barrier_semaphore()

    def greet_ep(d, carry):
        pl.semaphore_signal(barrier, inc=1, device_id={"ep": ep_peer(d)}, device_id_type=MESH)
        return carry

    def greet_z(d, carry):
        pl.semaphore_signal(
            barrier, inc=1, device_id={"tp": 2 * z_peer(d) + core}, device_id_type=MESH
        )
        return carry

    lax.fori_loop(1, n_ep, greet_ep, 0)
    lax.fori_loop(1, nz, greet_z, 0)
    pl.semaphore_signal(barrier, inc=1, device_id={"tp": partner}, device_id_type=MESH)
    pl.semaphore_wait(barrier, n_ep - 1 + nz - 1 + 1)

    def each(start, stop, fn):
        def run(d, carry):
            fn(d)
            return carry

        lax.fori_loop(start, stop, run, 0)

    each(1, nz, lambda d: osl_copy(z, z_peer(d)).start())
    for a in range(3):
        for direction in range(2):
            first_copy(direction, a).start()
    each(1, n_ep, lambda d: og_copy(ep, ep_peer(d)).start())

    def send_kv(d):
        kv_copy(ep, ep + d).start()
        ck_copy(ep, ep + d).start()

    each(1, n_ep - ep, send_kv)

    x[0, ep] = og_ref[ep]
    osl[z] = ow_ref[:, my_cols]

    attend_block(q_ref, cq_ref, kv_ref, ck_ref, m_ref, l_ref, att_acc, True)

    def attend_step(k):
        @pl.when(k <= ep)
        def _():
            j = ep - k
            kv_copy(j, j).wait_recv()
            ck_copy(j, j).wait_recv()
            attend_block(
                q_ref, cq_ref, kv_all.at[j], ck_all.at[j], m_ref, l_ref, att_acc, False
            )

    def expert_step(g_ref, u_ref, d_ref, first):
        for half in range(2):
            rows = x[half].reshape(n_ep * SLOT, width)
            g = jnp.dot(rows, g_ref[...], preferred_element_type=jnp.float32)
            u = jnp.dot(rows, u_ref[...], preferred_element_type=jnp.float32)
            part = jnp.dot(activate(g, u), d_ref[...], preferred_element_type=jnp.float32)
            if first:
                acc[half] = part
            else:
                acc[half] += part

    per_step = -(-n_ep // (3 * hops))

    def hop_step(h, carry):
        for a in range(3):
            for direction in range(2):
                @pl.when(h == 0)
                def _():
                    first_copy(direction, a).wait_recv()

                @pl.when(h > 0)
                def _():
                    ring_copy(direction, h, a).wait_recv()

                @pl.when(h < hops - 1)
                def _():
                    ring_copy(direction, h + 1, a).start()

                if (direction, a) in last_parts:
                    @pl.when(h == hops - 1)
                    def _():
                        last_copy(direction, a).start()

            if a == 1:
                @pl.when(h == 0)
                def _():
                    each(1, n_ep, lambda d: og_copy(ep_peer(d), ep_peer(d)).wait_recv())
                    pt_copy(x.at[0], x.at[1], 0).start()

            if a == 2:
                @pl.when(h == 0)
                def _():
                    each(1, nz, lambda d: osl_copy(z_peer(d), z_peer(d)).wait_recv())
                    each(1, n_ep, lambda d: w_copy(ep, ep_peer(d)).start())
                    w_all[ep] = osl[...]

            for i in range(per_step):
                attend_step((h * 3 + a) * per_step + i + 1)

        @pl.when(h == 0)
        def _():
            pt_copy(x.at[0], x.at[1], 0).wait_recv()
            expert_step(wg_ref, wu_ref, wd_ref, True)

        for direction in range(2):
            expert_step(
                rg.at[direction, h], ru.at[direction, h], rd.at[direction, h], False
            )
        return carry

    lax.fori_loop(0, hops, hop_step, 0)

    for pz in range(nz):
        rows = pl.ds(pz * 2 * t_dev, 2 * t_dev)
        o = (att_acc[rows, :] / l_ref[rows, :])[:, HEAD:]
        att_send[pz] = jnp.concatenate([o[:t_dev], o[t_dev:]], axis=1).astype(jnp.bfloat16)
    each(1, nz, lambda d: att_copy(z, z_peer(d)).start())
    att_in[z] = att_send[z]
    each(1, nz, lambda d: att_copy(z_peer(d), z_peer(d)).wait_recv())
    each(1, n_ep, lambda d: w_copy(ep_peer(d), ep_peer(d)).wait_recv())
    got = [att_in[pz].astype(jnp.float32) for pz in range(nz)]
    heads = jnp.concatenate(
        [
            jnp.concatenate([t[:, :HEAD] for t in got], axis=1),
            jnp.concatenate([t[:, HEAD:] for t in got], axis=1),
        ],
        axis=0,
    ).astype(jnp.bfloat16)

    def project(e, carry):
        piece = w_all[e].reshape(nz * HEAD, col)
        mix_acc[:, pl.ds(pl.multiple_of(e * col, col), col)] = jnp.dot(
            heads, piece, preferred_element_type=jnp.float32
        )
        return carry

    lax.fori_loop(0, n_ep, project, 0)
    theirs = pl.ds(pl.multiple_of((1 - core) * t_dev, t_dev), t_dev)
    mine = pl.ds(pl.multiple_of(core * t_dev, t_dev), t_dev)
    mp_send[...] = mix_acc[theirs, :].astype(jnp.bfloat16)
    pt_copy(mp_send, mp_recv, 1).start()

    last_copy(0, 0).wait_recv()
    last_copy(1, 1).wait_recv()
    acts = []
    for half in (1, 0):
        rows = x[half].reshape(n_ep * SLOT, width)
        g = jnp.dot(rows, lg[...], preferred_element_type=jnp.float32)
        u = jnp.dot(rows, lu[...], preferred_element_type=jnp.float32)
        acts.append(activate(g, u))
    pt_copy(mp_send, mp_recv, 1).wait_recv()
    mix_ref[...] = (mix_acc[mine, :] + mp_recv[...].astype(jnp.float32)).astype(jnp.bfloat16)
    last_copy(0, 2).wait_recv()
    last_copy(1, 2).wait_recv()
    p_send[...] = (
        acc[1] + jnp.dot(acts[0], ld[...], preferred_element_type=jnp.float32)
    ).astype(jnp.bfloat16)
    pt_copy(p_send, p_recv, 2).start()
    acc[0] += jnp.dot(acts[1], ld[...], preferred_element_type=jnp.float32)
    pt_copy(p_send, p_recv, 2).wait_recv()
    res[...] = (
        (acc[0] + p_recv[...].astype(jnp.float32))
        .astype(jnp.bfloat16)
        .reshape(n_ep, SLOT, width)
    )
    each(1, n_ep, lambda d: res_copy(ep, ep_peer(d)).start())
    ret[ep] = res[ep]

    each(1, nz, lambda d: osl_copy(z, z_peer(d)).wait_send())
    each(1, nz, lambda d: att_copy(z, z_peer(d)).wait_send())
    for a in range(3):
        for direction in range(2):
            first_copy(direction, a).wait_send()
            each(1, hops, lambda h: ring_copy(direction, h, a).wait_send())
    for direction, a in last_parts:
        last_copy(direction, a).wait_send()
    each(1, n_ep, lambda d: og_copy(ep, ep_peer(d)).wait_send())
    each(1, n_ep, lambda d: w_copy(ep, ep_peer(d)).wait_send())

    def sent_kv(d):
        kv_copy(ep, ep + d).wait_send()
        ck_copy(ep, ep + d).wait_send()

    each(1, n_ep - ep, sent_kv)
    pt_copy(x.at[0], x.at[1], 0).wait_send()
    pt_copy(mp_send, mp_recv, 1).wait_send()
    pt_copy(p_send, p_recv, 2).wait_send()

    each(1, n_ep, lambda d: res_copy(ep_peer(d), ep_peer(d)).wait_recv())
    c0 = comb_ref[...]
    c_hi = c0.astype(jnp.bfloat16)
    c1 = c0 - c_hi.astype(jnp.float32)
    c_mid = c1.astype(jnp.bfloat16)
    c_lo = (c1 - c_mid.astype(jnp.float32)).astype(jnp.bfloat16)
    back = ret[...].reshape(n_ep * SLOT, width)
    total = jnp.dot(c_hi, back, preferred_element_type=jnp.float32)
    total += jnp.dot(c_mid, back, preferred_element_type=jnp.float32)
    total += jnp.dot(c_lo, back, preferred_element_type=jnp.float32)
    eo_ref[...] = total.astype(jnp.bfloat16)
    each(1, n_ep, lambda d: res_copy(ep, ep_peer(d)).wait_send())


def route(expert_choice, route_weights, n_experts):
    flat_ids = expert_choice.reshape(-1)
    one_hot = (flat_ids[:, None] == jnp.arange(n_experts, dtype=jnp.int32)[None, :]).astype(
        jnp.int32
    )
    slot_rank = jnp.sum((jnp.cumsum(one_hot, axis=0) - one_hot) * one_hot, axis=1)
    slot_ids = (flat_ids * SLOT + slot_rank).reshape(expert_choice.shape)
    table = slot_ids[:, :, None] == jnp.arange(n_experts * SLOT, dtype=jnp.int32)[None, None, :]
    placing = jnp.sum(table.astype(jnp.bfloat16), axis=1)
    combine = jnp.sum(jnp.where(table, route_weights[:, :, None], 0.0), axis=1)
    return placing, combine


def local(
    n_ep,
    n_tp,
    queries,
    key_vectors,
    value_vectors,
    cumulative_gate,
    out_weight,
    expert_tokens,
    norm_gain,
    gate_weight,
    up_weight,
    down_weight,
    expert_choice,
    route_weights,
):
    tokens, width = expert_tokens.shape
    block, head = queries.shape
    units = gate_weight.shape[2]
    nz = n_tp // 2
    hops = nz // 2 - 1
    t_dev = block // n_tp
    col = width // n_ep
    bf16, f32 = jnp.bfloat16, jnp.float32

    tokens_float = expert_tokens.astype(f32)
    normed = (
        tokens_float
        * lax.rsqrt(jnp.mean(tokens_float * tokens_float, axis=1, keepdims=True) + eps_norm)
        * norm_gain
    ).astype(bf16)
    placing, combine = route(expert_choice, route_weights, n_ep)
    outgoing = (
        jnp.einsum("ts,td->sd", placing, normed, preferred_element_type=f32)
        .astype(bf16)
        .reshape(n_ep, SLOT, width)
    )
    kv = jnp.concatenate([key_vectors, value_vectors], axis=1)
    gate_tile = cumulative_gate.reshape(block // 128, 128)
    q_wide = jnp.pad(queries * bf16(1.0 / math.sqrt(head)), ((0, 0), (0, 128 - head)))

    dma = pltpu.SemaphoreType.DMA
    vmem = pltpu.VMEM
    mixer, experts = pl.pallas_call(
        functools.partial(body, n_ep, n_tp),
        out_shape=(
            jax.ShapeDtypeStruct((t_dev, width), bf16),
            jax.ShapeDtypeStruct((tokens, width), bf16),
        ),
        in_specs=[pl.BlockSpec(memory_space=vmem)] * 10,
        out_specs=(pl.BlockSpec(memory_space=vmem),) * 2,
        scratch_shapes=[
            vmem((n_ep, block, 128), bf16),
            vmem((n_ep, block // 128, 128), f32),
            vmem((2, hops, width, units), bf16),
            vmem((2, hops, width, units), bf16),
            vmem((2, hops, units, width), bf16),
            vmem((width, units), bf16),
            vmem((width, units), bf16),
            vmem((units, width), bf16),
            vmem((2, n_ep, SLOT, width), bf16),
            vmem((2, n_ep * SLOT, width), f32),
            vmem((n_ep * SLOT, width), bf16),
            vmem((n_ep * SLOT, width), bf16),
            vmem((n_ep, SLOT, width), bf16),
            vmem((n_ep, SLOT, width), bf16),
            vmem((nz, head, col), bf16),
            vmem((n_ep, nz, head, col), bf16),
            vmem((nz, t_dev, 128), bf16),
            vmem((nz, t_dev, 128), bf16),
            vmem((2 * t_dev, width), f32),
            vmem((t_dev, width), bf16),
            vmem((t_dev, width), bf16),
            vmem((block, 128), f32),
            vmem((block, 128), f32),
            vmem((block, 128), f32),
        ]
        + [dma((n_ep,))] * 8
        + [dma((nz,))] * 2
        + [dma((n_ep,))] * 2
        + [dma((nz,))] * 2
        + [dma((2, hops + 1, 3))] * 2
        + [dma((3,))] * 2,
        compiler_params=pltpu.CompilerParams(
            collective_id=0, has_side_effects=True, vmem_limit_bytes=63 * 2**20
        ),
        name="whole",
    )(
        q_wide,
        cumulative_gate,
        kv,
        gate_tile,
        gate_weight[0],
        up_weight[0],
        down_weight[0],
        out_weight,
        outgoing,
        combine,
    )
    return mixer, experts


def solution(mesh):
    placed = (
        P("ep", "tp"),
        P("ep", "tp"),
        P("ep", "tp"),
        P("ep", "tp"),
        P("tp", None),
        P(("ep", "tp"), None),
        P(),
        P("ep", None, "tp"),
        P("ep", None, "tp"),
        P("ep", "tp", None),
        P(("ep", "tp"), None),
        P(("ep", "tp"), None),
    )
    return jax.shard_map(
        functools.partial(local, mesh.shape["ep"], mesh.shape["tp"]),
        mesh=mesh,
        in_specs=placed,
        out_specs=(P(("ep", "tp"), None), P(("ep", "tp"), None)),
        check_vma=False,
    )
```

time: 310 us -> 192 us (0.62)
  waiting for transfers between devices: 190 us -> 0 us
  Pallas kernels: 25.9 us -> 173 us
  blocking collectives: 29.5 us -> 0 us
  starting transfers between devices: 22.2 us -> 0 us
  between operations: 13.9 us -> 0.75 us
  local copies, waits for them, and re-layouts: 15.2 us -> 8.01 us
  matrix products: 7.61 us -> 1.5 us
    all_gather x5 -> x0, waiting for transfers between devices: 185 us -> none  [the longest x1 56.8 us: local(): down_all = lax.all_gather(down_weight[0], 'tp', axis=0, tiled=True)]
    pallas_call x2 -> x1, Pallas kernels: 25.9 us -> 173 us  [local(): pl.pallas_call(functools.partial(body, n_ep, n_tp), out_shape=(jax.ShapeD...]
    all_gather x1 -> x0, blocking collectives: 29.5 us -> none  [local(): gates_all = lax.all_gather(gate_tile, 'ep', axis=0)]
    all_to_all x3 -> x0, starting transfers between devices: 22 us -> none  [the longest x1 7.86 us: local(): lax.all_to_all(attention.reshape(n_tp, block_rows // n_tp, head), 'tp', s...]
    all_gather x1 -> x0, local copies, waits for them, and re-layouts: 6.43 us -> none  [local(): lax.all_gather(kv, 'ep', axis=0, tiled=True).reshape(n_ep, block_rows, 128)]
    dot_general x3 -> x1, matrix products: 7.61 us -> 1.5 us  [local(): jnp.einsum('ts,td->sd', placing, normed, preferred_element_type=f32)]
    all_to_all x3 -> x0, waiting for transfers between devices: 3.19 us -> none  [the longest x1 3.19 us: local(): lax.all_to_all(results.reshape(n_ep, SLOT, width), 'ep', split_axis=0, co...]
    unnamed x15 -> x17, local copies, waits for them, and re-layouts: 7.86 us -> 6.73 us
  transfers between devices with their start and end apart: 8 -> 0, of which waited for: 6 -> 0; matrix products, arithmetic and copies ran while one was open for 6% -> 0% of each run, Pallas kernels for 8% -> 0%
where the time goes in v1:
time: 192 us; the launch traced here: 189 us
  Pallas kernels  173 us (90%)
  local copies, waits for them, and re-layouts  8.01 us (4%)
  other arithmetic  5.04 us (3%)
    pallas_call x1, Pallas kernels, local(): pl.pallas_call(functools.partial(body, n_ep, n_tp), out_shape=(jax.ShapeD...  173 us
    unnamed x17, local copies, waits for them, and re-layouts  6.73 us

profile of v1, /device:TPU:1, one launch (start us, length us, event | category | flops | bytes accessed | tf_op | source)
XLA Modules:
  0.0 188.6 jit_solution(4712317446110504994)
XLA Ops:
  0.6 1.2 fusion
  1.8 0.0 copy-start.1
  1.8 0.8 copy.44
  2.6 0.1 eq.35
  2.8 0.6 reduce-window.6
  3.4 0.2 slice_reduce_fusion
  3.6 0.1 bitcast_bitcast_fusion
  3.7 0.0 copy-start.2
  3.7 0.1 reduce_sum.42
  3.9 0.1 copy.47
  3.9 0.7 multiply_add_fusion
  4.7 0.1 fusion.7
  4.8 1.4 select_reduce_fusion.comb_ref
  6.2 1.1 copy.40
  7.3 0.0 copy-start.3
  7.3 0.8 pad.8.q_ref
  8.1 0.0 copy-done.1
  8.1 0.0 copy-start
  8.1 0.0 copy-start.4
  8.1 0.2 copy.42
  8.3 0.0 copy-done.2
  8.3 0.2 copy.43
  8.4 0.9 pad_maximum_fusion.kv_ref
  9.3 0.0 copy-done.3
  9.3 1.0 copy.48.cq_ref
  10.3 0.0 copy-done
  10.3 0.0 copy-done.4
  10.4 1.5 convolution_convert_fusion
  11.8 173.3 %whole.1 = (bf16[64,2048]{1,0:T(8,128)(2,1)}, bf16[96,2048]{1,0:T(8,128)(2,1)}) custom-call(bf16[1024,128]{1,0:T(8,128)(2,1)} %pad.8.q_ref, f32[1024,1]{1,0:T(8,128)} %copy.48.cq_ref, bf16[1024,128]{1,0:T(8,128)(2,1)} %pad_maximum_fusion.kv_ref, f32[8,128]{1,0:T(8,128)} %bitcast.22, bf16[2048,128]{1,0:T(8,128)(2,1)} %bitcast.19, bf16[2048,128]{1,0:T(8,128)(2,1)} %bitcast.20, ...), custom_call_target="tpu_custom_call" | custom-call | tf_op jit(solution)/shard_map/whole/pallas_call | solution.py:482
  185.1 1.7 copy.55
  186.8 1.8 copy.56
  (7 shorter events, 0.1 us)
Async XLA Ops:
  1.8 6.3 %copy-start.1 = (bf16[1024,64]{0,1:T(8,128)(2,1)S(1)}, bf16[1024,64]{0,1:T(8,128)(2,1)}, u32[]{:S(2)}) copy-start(bf16[1024,64]{0,1:T(8,128)(2,1)} %param.13) | copy-start | bytes 393220
  3.7 4.5 %copy-start.2 = (bf16[1024,64]{0,1:T(8,128)(2,1)S(1)}, bf16[1024,64]{0,1:T(8,128)(2,1)}, u32[]{:S(2)}) copy-start(bf16[1024,64]{0,1:T(8,128)(2,1)} %param.14) | copy-start | bytes 393220
  7.3 2.0 %copy-start.3 = (f32[1024,1]{0,1:T(1,128)S(1)}, f32[1024,1]{0,1:T(1,128)}, u32[]{:S(2)}) copy-start(f32[1024,1]{0,1:T(1,128)} %param.15) | copy-start | bytes 12292
  8.1 2.3 %copy-start = (bf16[96,2048]{1,0:T(8,128)(2,1)S(1)}, bf16[96,2048]{1,0:T(8,128)(2,1)}, u32[]{:S(2)}) copy-start(bf16[96,2048]{1,0:T(8,128)(2,1)} %param.17) | copy-start | bytes 1179652
  8.1 2.3 %copy-start.4 = (f32[2048]{0:T(1024)S(1)}, f32[2048]{0:T(1024)}, u32[]{:S(2)}) copy-start(f32[2048]{0:T(1024)} %param.18) | copy-start | bytes 24580

commit v2 on v1

v2 whole, which is shorter than its diff:
```python
import functools
import math

import jax
import jax.numpy as jnp
from jax import lax
from jax.experimental import pallas as pl
from jax.experimental.pallas import tpu as pltpu
from jax.sharding import PartitionSpec as P

SLOT = 16
TQ = 256
HEAD = 64
MESH = pl.DeviceIdType.MESH

eps_norm = 1e-05
clamp_limit = 7.0
sig_alpha = 1.702
floor_score = -1e30


def gate_row(tile):
    return jnp.concatenate([tile[r : r + 1, :] for r in range(tile.shape[0])], axis=1)


def activate(g, u):
    g = jnp.minimum(g, clamp_limit)
    u = jnp.clip(u, -clamp_limit, clamp_limit)
    return (g * jax.nn.sigmoid(sig_alpha * g) * (u + 1.0)).astype(jnp.bfloat16)


def attend_block(q_ref, cq_ref, kv_ref, ck_ref, m_ref, l_ref, acc_ref, diagonal):
    width = kv_ref.shape[0]
    tile = min(TQ, q_ref.shape[0])
    ck_row = gate_row(ck_ref[...])

    def one_tile(i, carry):
        rows = pl.ds(pl.multiple_of(i * tile, tile), tile)
        kv = kv_ref[...]
        s = lax.dot_general(
            q_ref[rows, :], kv, (((1,), (1,)), ((), ())), preferred_element_type=jnp.float32
        )
        s = s + (cq_ref[rows, :] - ck_row)
        if diagonal:
            q_pos = i * tile + lax.broadcasted_iota(jnp.int32, (tile, width), 0)
            k_pos = lax.broadcasted_iota(jnp.int32, (tile, width), 1)
            s = jnp.where(k_pos <= q_pos, s, floor_score)
        top = jnp.max(s, axis=1, keepdims=True)
        if diagonal:
            p = jnp.exp(s - top)
            m_ref[rows, :] = jnp.broadcast_to(top, (tile, 128))
            l_ref[rows, :] = jnp.broadcast_to(jnp.sum(p, axis=1, keepdims=True), (tile, 128))
            acc_ref[rows, :] = jnp.dot(
                p.astype(jnp.bfloat16), kv, preferred_element_type=jnp.float32
            )
        else:
            old = m_ref[rows, :]
            new = jnp.maximum(old, top)
            shrink = jnp.exp(old - new)
            p = jnp.exp(s - new[:, :1])
            m_ref[rows, :] = new
            l_ref[rows, :] = l_ref[rows, :] * shrink + jnp.sum(p, axis=1, keepdims=True)
            acc_ref[rows, :] = acc_ref[rows, :] * shrink + jnp.dot(
                p.astype(jnp.bfloat16), kv, preferred_element_type=jnp.float32
            )
        return carry

    lax.fori_loop(0, q_ref.shape[0] // tile, one_tile, 0)


N_BLOCKS = 4
DOWN_ORDER = {
    3: ((0, 0), (1, 0), (2, 0), (0, 1), (1, 1), (0, 2), (2, 1), (0, 3), (1, 2), (3, 0),
        (1, 3), (2, 2), (3, 1), (2, 3), (3, 2), (3, 3)),
    1: ((0, 0), (1, 0), (2, 0), (0, 1), (1, 1), (3, 0), (2, 1), (3, 1)),
}


def body(
    n_ep,
    n_tp,
    qt_ref,
    kt_ref,
    vt_ref,
    ck_ref,
    wg_ref,
    wu_ref,
    wd_ref,
    ow_ref,
    tok_ref,
    gain_ref,
    choice_ref,
    route_ref,
    mix_ref,
    eo_ref,
    q_ref,
    cq_ref,
    kv_ref,
    og_ref,
    comb_ref,
    kv_all,
    ck_all,
    rg,
    ru,
    lg,
    lu,
    dn,
    act,
    x,
    acc,
    p_send,
    p_recv,
    res,
    ret,
    osl,
    w_all,
    att_send,
    att_in,
    heads_ref,
    mix_acc,
    mp_send,
    mp_recv,
    m_ref,
    l_ref,
    att_acc,
    s_kv,
    r_kv,
    s_ck,
    r_ck,
    s_og,
    r_og,
    s_w,
    r_w,
    s_osl,
    r_osl,
    s_att,
    r_att,
    s_res,
    r_res,
    s_ring,
    r_ring,
    s_pt,
    r_pt,
):
    bf16, f32 = jnp.bfloat16, jnp.float32
    nz = n_tp // 2
    hops = nz // 2 - 1
    ep = lax.axis_index("ep")
    tp = lax.axis_index("tp")
    z = lax.div(tp, 2)
    core = lax.rem(tp, 2)
    right = lax.rem(tp + 2, n_tp)
    left = lax.rem(tp + n_tp - 2, n_tp)
    partner = tp + 1 - 2 * core
    units, width = wd_ref.shape
    block = q_ref.shape[0]
    tokens = tok_ref.shape[0]
    slots_all = n_ep * SLOT
    col = width // n_ep
    part = width // N_BLOCKS
    t_dev = mp_send.shape[0]

    def ep_peer(d):
        return lax.rem(ep + d, n_ep)

    def z_peer(d):
        return lax.rem(z + d, nz)

    def ep_copy(src, dst, send, recv, peer):
        return pltpu.make_async_remote_copy(
            src_ref=src, dst_ref=dst, send_sem=send, recv_sem=recv,
            device_id={"ep": peer}, device_id_type=MESH,
        )

    def tp_copy(src, dst, send, recv, peer):
        return pltpu.make_async_remote_copy(
            src_ref=src, dst_ref=dst, send_sem=send, recv_sem=recv,
            device_id={"tp": peer}, device_id_type=MESH,
        )

    def kv_copy(slot, peer):
        return ep_copy(kv_ref, kv_all.at[slot], s_kv.at[peer], r_kv.at[slot], peer)

    def ck_copy(slot, peer):
        return ep_copy(ck_ref, ck_all.at[slot], s_ck.at[peer], r_ck.at[slot], peer)

    def og_copy(slot, peer):
        return ep_copy(og_ref.at[peer], x.at[0, slot], s_og.at[peer], r_og.at[slot], peer)

    def res_copy(b, slot, peer):
        return ep_copy(
            res.at[b, peer], ret.at[b, slot], s_res.at[b, peer], r_res.at[b, slot], peer
        )

    def w_copy(slot, peer):
        return ep_copy(osl, w_all.at[slot], s_w.at[peer], r_w.at[slot], peer)

    my_cols = pl.ds(pl.multiple_of(ep * col, col), col)

    def osl_copy(slot, pz):
        return tp_copy(
            ow_ref.at[:, my_cols], osl.at[slot], s_osl.at[pz], r_osl.at[slot], 2 * pz + core
        )

    def att_copy(slot, pz):
        return tp_copy(
            att_send.at[pz], att_in.at[slot], s_att.at[pz], r_att.at[slot], 2 * pz + core
        )

    def pt_copy(src, dst, n):
        return tp_copy(src, dst, s_pt.at[n], r_pt.at[n], partner)

    def x_copy():
        return pt_copy(x.at[0], x.at[1], 0)

    def mp_copy():
        return pt_copy(mp_send, mp_recv, 1)

    def p_copy(b):
        return pt_copy(p_send.at[b], p_recv.at[b], 2 + b)

    peers = (right, left)
    own = (wg_ref, wu_ref)
    slots = (rg, ru)
    last = (lg, lu)
    firsts = 2 * hops + 1
    down_order = DOWN_ORDER[hops]
    items = firsts + len(down_order)

    def gu_copy(direction, h, j):
        a = j if direction == 0 else 1 - j
        n = 2 * h + j
        sems = (s_ring.at[direction, n], r_ring.at[direction, n])
        return lambda src, dst: tp_copy(src, dst, *sems, peers[direction]), a

    def gu_first(direction, j):
        make, a = gu_copy(direction, 0, j)
        return make(own[a], slots[a].at[direction, 0])

    def gu_next(direction, h, j):
        make, a = gu_copy(direction, h, j)
        return make(slots[a].at[direction, h - 1], slots[a].at[direction, h])

    def gu_last(direction):
        make, a = gu_copy(direction, hops, 0)
        return make(slots[a].at[direction, hops - 1], last[a])

    def down_copy(direction, i):
        b, h = down_order[i]
        cols = pl.ds(b * part, part)
        n = firsts + i
        rows = pl.ds(0, units)
        to = 1 + 2 * h + direction
        if h == hops:
            rows = pl.ds(direction * (units // 2), units // 2)
            to = 1 + 2 * hops
        if h == 0:
            src = wd_ref.at[rows, cols]
        else:
            src = dn.at[1 + 2 * (h - 1) + direction, rows, cols]
        return tp_copy(
            src, dn.at[to, rows, cols], s_ring.at[direction, n], r_ring.at[direction, n],
            peers[direction],
        )

    def start_down(i):
        for direction in range(2):
            down_copy(direction, i).start()

    def each(start, stop, fn):
        def run(d, carry):
            fn(d)
            return carry

        lax.fori_loop(start, stop, run, 0)

    barrier = pltpu.get_barrier_semaphore()
    each(
        1, n_ep,
        lambda d: pl.semaphore_signal(
            barrier, inc=1, device_id={"ep": ep_peer(d)}, device_id_type=MESH
        ),
    )
    each(
        1, nz,
        lambda d: pl.semaphore_signal(
            barrier, inc=1, device_id={"tp": 2 * z_peer(d) + core}, device_id_type=MESH
        ),
    )
    pl.semaphore_signal(barrier, inc=1, device_id={"tp": partner}, device_id_type=MESH)
    pl.semaphore_wait(barrier, n_ep - 1 + nz - 1 + 1)

    for j in range(2):
        for direction in range(2):
            gu_first(direction, j).start()
    each(1, nz, lambda d: osl_copy(z, z_peer(d)).start())

    kv_ref[...] = (
        jnp.concatenate([kt_ref[...].astype(f32), vt_ref[...].astype(f32)], axis=0)
        .T.astype(bf16)
    )
    scaled = qt_ref[...].astype(f32) * (1.0 / math.sqrt(HEAD))
    q_ref[...] = jnp.concatenate([scaled, jnp.zeros_like(scaled)], axis=0).T.astype(bf16)
    turned = ck_ref[...].T
    for r in range(block // 128):
        cq_ref[pl.ds(r * 128, 128), :] = turned[:, r : r + 1]

    ids = choice_ref[...]
    e_pos = lax.broadcasted_iota(jnp.int32, (n_ep, tokens), 0)
    named = [(e_pos == ids[k : k + 1, :]).astype(f32) for k in range(ids.shape[0])]
    both = functools.reduce(jnp.add, named)
    before = (
        lax.broadcasted_iota(jnp.int32, (tokens, tokens), 0)
        < lax.broadcasted_iota(jnp.int32, (tokens, tokens), 1)
    )
    earlier = jnp.dot(
        both.astype(bf16), before.astype(f32).astype(bf16), preferred_element_type=f32
    )
    s_pos = lax.broadcasted_iota(jnp.int32, (slots_all, tokens), 0).astype(f32)
    placing = jnp.zeros((slots_all, tokens), f32)
    comb = jnp.zeros((slots_all, tokens), f32)
    for k in range(ids.shape[0]):
        rank = jnp.sum(named[k] * earlier, axis=0, keepdims=True)
        slot = ids[k : k + 1, :].astype(f32) * SLOT + rank
        here = s_pos == slot
        placing = jnp.where(here, 1.0, placing)
        comb = jnp.where(here, route_ref[k : k + 1, :], comb)
    comb_ref[...] = comb.T
    tok = tok_ref[...].astype(f32)
    normed = (
        tok * lax.rsqrt(jnp.mean(tok * tok, axis=1, keepdims=True) + eps_norm) * gain_ref[...]
    ).astype(bf16)
    og_ref[...] = (
        jnp.dot(placing.astype(bf16), normed, preferred_element_type=f32)
        .astype(bf16)
        .reshape(n_ep, SLOT, width)
    )

    attend_block(q_ref, cq_ref, kv_ref, ck_ref, m_ref, l_ref, att_acc, True)

    def send_kv(d):
        kv_copy(ep, ep + d).start()
        ck_copy(ep, ep + d).start()

    near = jnp.minimum(n_ep - ep, 4)
    each(1, near, send_kv)
    each(1, n_ep, lambda d: og_copy(ep, ep_peer(d)).start())
    each(near, n_ep - ep, send_kv)
    x[0, ep] = og_ref[ep]
    osl[z] = ow_ref[:, my_cols]
    dn[0] = wd_ref[...]

    def attend_step(k):
        j = ep - k
        kv_copy(j, j).wait_recv()
        ck_copy(j, j).wait_recv()
        attend_block(q_ref, cq_ref, kv_all.at[j], ck_all.at[j], m_ref, l_ref, att_acc, False)

    def expert_units(g_ref, u_ref, n):
        cols = pl.ds(pl.multiple_of(n * units, units), units)
        for half in range(2):
            rows = x[half].reshape(slots_all, width)
            g = jnp.dot(rows, g_ref[...], preferred_element_type=f32)
            u = jnp.dot(rows, u_ref[...], preferred_element_type=f32)
            act[half, :, cols] = activate(g, u)

    per_step = -(-(n_ep - 1) // (2 * hops - 1))

    def hop_step(h, carry):
        for j in range(2):
            for direction in range(2):
                @pl.when(h == 0)
                def _():
                    gu_first(direction, j).wait_recv()

                @pl.when(h > 0)
                def _():
                    gu_next(direction, h, j).wait_recv()

                @pl.when(h < hops - 1)
                def _():
                    gu_next(direction, h + 1, j).start()

                if j == 0:
                    @pl.when(h == hops - 1)
                    def _():
                        gu_last(direction).start()

            if j == 1:
                @pl.when(h == hops - 1)
                def _():
                    for i in range(3):
                        start_down(i)

                @pl.when(h == 0)
                def _():
                    each(1, n_ep, lambda d: og_copy(ep_peer(d), ep_peer(d)).wait_recv())
                    x_copy().start()
                    each(1, nz, lambda d: osl_copy(z_peer(d), z_peer(d)).wait_recv())
                    each(1, n_ep, lambda d: w_copy(ep, ep_peer(d)).start())
                    w_all[ep] = osl[...]

            k0 = (2 * h + j) * per_step + 1
            each(k0, jnp.minimum(k0 + per_step, ep + 1), attend_step)

        @pl.when(h == 0)
        def _():
            x_copy().wait_recv()
            expert_units(wg_ref, wu_ref, 0)

        for direction in range(2):
            expert_units(rg.at[direction, h], ru.at[direction, h], 1 + 2 * h + direction)
        return carry

    lax.fori_loop(0, hops, hop_step, 0)

    for pz in range(nz):
        rows = pl.ds(pz * 2 * t_dev, 2 * t_dev)
        o = (att_acc[rows, :] / l_ref[rows, :])[:, HEAD:]
        att_send[pz] = jnp.concatenate([o[:t_dev], o[t_dev:]], axis=1).astype(bf16)
    for direction in range(2):
        gu_last(direction).wait_recv()
    each(1, nz, lambda d: att_copy(z, z_peer(d)).start())
    att_in[z] = att_send[z]
    expert_units(lg, lu, 1 + 2 * hops)

    def gather_heads():
        each(1, nz, lambda d: att_copy(z_peer(d), z_peer(d)).wait_recv())
        got = [att_in[pz].astype(f32) for pz in range(nz)]
        heads_ref[pl.ds(0, t_dev), :] = jnp.concatenate(
            [t[:, :HEAD] for t in got], axis=1
        ).astype(bf16)
        heads_ref[pl.ds(t_dev, t_dev), :] = jnp.concatenate(
            [t[:, HEAD:] for t in got], axis=1
        ).astype(bf16)
        each(1, n_ep, lambda d: w_copy(ep_peer(d), ep_peer(d)).wait_recv())

    def project(e):
        piece = w_all[e].reshape(nz * HEAD, col)
        mix_acc[:, pl.ds(pl.multiple_of(e * col, col), col)] = jnp.dot(
            heads_ref[...], piece, preferred_element_type=f32
        )

    theirs = pl.ds(pl.multiple_of((1 - core) * t_dev, t_dev), t_dev)
    mine = pl.ds(pl.multiple_of(core * t_dev, t_dev), t_dev)

    def send_mix():
        mp_send[...] = mix_acc[theirs, :].astype(bf16)
        mp_copy().start()

    def take_mix():
        mp_copy().wait_recv()
        mix_ref[...] = (mix_acc[mine, :] + mp_recv[...].astype(f32)).astype(bf16)

    def finish_units(b):
        weights = dn[:, :, b * part : (b + 1) * part].reshape(nz * units, part)
        p_send[b] = jnp.dot(act[1], weights, preferred_element_type=f32).astype(bf16)
        p_copy(b).start()
        acc[b] = jnp.dot(act[0], weights, preferred_element_type=f32)

    def send_home(b):
        p_copy(b).wait_recv()
        res[b] = (acc[b] + p_recv[b].astype(f32)).astype(bf16).reshape(n_ep, SLOT, part)
        each(1, n_ep, lambda d: res_copy(b, ep, ep_peer(d)).start())
        ret[b, ep] = res[b, ep]

    c0 = comb_ref[...]
    c_hi = c0.astype(bf16)
    c1 = c0 - c_hi.astype(f32)
    c_mid = c1.astype(bf16)
    c_lo = (c1 - c_mid.astype(f32)).astype(bf16)

    def combine(b):
        each(1, n_ep, lambda d: res_copy(b, ep_peer(d), ep_peer(d)).wait_recv())
        back = ret[b].reshape(slots_all, part)
        total = jnp.dot(c_hi, back, preferred_element_type=f32)
        total += jnp.dot(c_mid, back, preferred_element_type=f32)
        total += jnp.dot(c_lo, back, preferred_element_type=f32)
        eo_ref[:, b * part : (b + 1) * part] = total.astype(bf16)

    count = len(down_order)
    issued = 3
    arrived = []
    pending = []
    mixer_work = [gather_heads]
    quarter = -(-n_ep // 4)
    for q in range(4):
        mixer_work.append(
            functools.partial(each, q * quarter, min((q + 1) * quarter, n_ep), project)
        )
    mixer_work += [send_mix, take_mix]
    mixer_at = min(4, count - 8) if count > 8 else 0
    for i in range(count):
        for direction in range(2):
            down_copy(direction, i).wait_recv()
        arrived.append(down_order[i])
        while issued < min(count, i + 3):
            b, h = down_order[issued]
            if h > 0 and (b, h - 1) not in arrived:
                break
            start_down(issued)
            issued += 1
        for b in pending:
            send_home(b)
        pending = []
        b, h = down_order[i]
        if h == hops:
            finish_units(b)
            pending.append(b)
        elif i >= mixer_at and mixer_work:
            mixer_work.pop(0)()
    for b in pending:
        send_home(b)
    for work in mixer_work:
        work()

    each(1, nz, lambda d: osl_copy(z, z_peer(d)).wait_send())
    each(1, nz, lambda d: att_copy(z, z_peer(d)).wait_send())
    for direction in range(2):
        for j in range(2):
            gu_first(direction, j).wait_send()
            each(1, hops, lambda h: gu_next(direction, h, j).wait_send())
        gu_last(direction).wait_send()
        for i in range(count):
            down_copy(direction, i).wait_send()
    each(1, n_ep, lambda d: og_copy(ep, ep_peer(d)).wait_send())
    each(1, n_ep, lambda d: w_copy(ep, ep_peer(d)).wait_send())

    def sent_kv(d):
        kv_copy(ep, ep + d).wait_send()
        ck_copy(ep, ep + d).wait_send()

    each(1, n_ep - ep, sent_kv)
    x_copy().wait_send()
    mp_copy().wait_send()
    for b in range(N_BLOCKS):
        p_copy(b).wait_send()
    for b in range(N_BLOCKS):
        combine(b)
    for b in range(N_BLOCKS):
        each(1, n_ep, lambda d: res_copy(b, ep, ep_peer(d)).wait_send())


def local(
    n_ep,
    n_tp,
    queries,
    key_vectors,
    value_vectors,
    cumulative_gate,
    out_weight,
    expert_tokens,
    norm_gain,
    gate_weight,
    up_weight,
    down_weight,
    expert_choice,
    route_weights,
):
    tokens, width = expert_tokens.shape
    block, head = queries.shape
    units = gate_weight.shape[2]
    nz = n_tp // 2
    hops = nz // 2 - 1
    t_dev = block // n_tp
    col = width // n_ep
    part = width // N_BLOCKS
    slots_all = n_ep * SLOT
    items = 2 * hops + 1 + len(DOWN_ORDER[hops])
    bf16, f32 = jnp.bfloat16, jnp.float32
    dma = pltpu.SemaphoreType.DMA
    vmem = pltpu.VMEM
    return pl.pallas_call(
        functools.partial(body, n_ep, n_tp),
        out_shape=(
            jax.ShapeDtypeStruct((t_dev, width), bf16),
            jax.ShapeDtypeStruct((tokens, width), bf16),
        ),
        in_specs=[pl.BlockSpec(memory_space=vmem)] * 12,
        out_specs=(pl.BlockSpec(memory_space=vmem),) * 2,
        scratch_shapes=[
            vmem((block, 128), bf16),
            vmem((block, 1), f32),
            vmem((block, 128), bf16),
            vmem((n_ep, SLOT, width), bf16),
            vmem((tokens, slots_all), f32),
            vmem((n_ep, block, 128), bf16),
            vmem((n_ep, block // 128, 128), f32),
            vmem((2, hops, width, units), bf16),
            vmem((2, hops, width, units), bf16),
            vmem((width, units), bf16),
            vmem((width, units), bf16),
            vmem((nz, units, width), bf16),
            vmem((2, slots_all, nz * units), bf16),
            vmem((2, n_ep, SLOT, width), bf16),
            vmem((N_BLOCKS, slots_all, part), f32),
            vmem((N_BLOCKS, slots_all, part), bf16),
            vmem((N_BLOCKS, slots_all, part), bf16),
            vmem((N_BLOCKS, n_ep, SLOT, part), bf16),
            vmem((N_BLOCKS, n_ep, SLOT, part), bf16),
            vmem((nz, head, col), bf16),
            vmem((n_ep, nz, head, col), bf16),
            vmem((nz, t_dev, 128), bf16),
            vmem((nz, t_dev, 128), bf16),
            vmem((2 * t_dev, nz * head), bf16),
            vmem((2 * t_dev, width), f32),
            vmem((t_dev, width), bf16),
            vmem((t_dev, width), bf16),
            vmem((block, 128), f32),
            vmem((block, 128), f32),
            vmem((block, 128), f32),
        ]
        + [dma((n_ep,))] * 8
        + [dma((nz,))] * 4
        + [dma((N_BLOCKS, n_ep))] * 2
        + [dma((2, items))] * 2
        + [dma((2 + N_BLOCKS,))] * 2,
        compiler_params=pltpu.CompilerParams(
            collective_id=0, has_side_effects=True, vmem_limit_bytes=60 * 2**20
        ),
        name="whole",
    )(
        queries.T,
        key_vectors.T,
        value_vectors.T,
        cumulative_gate.reshape(block // 128, 128),
        gate_weight[0],
        up_weight[0],
        down_weight[0],
        out_weight,
        expert_tokens,
        norm_gain.reshape(1, width),
        expert_choice.T,
        route_weights.T,
    )


def solution(mesh):
    placed = (
        P("ep", "tp"),
        P("ep", "tp"),
        P("ep", "tp"),
        P("ep", "tp"),
        P("tp", None),
        P(("ep", "tp"), None),
        P(),
        P("ep", None, "tp"),
        P("ep", None, "tp"),
        P("ep", "tp", None),
        P(("ep", "tp"), None),
        P(("ep", "tp"), None),
    )
    return jax.shard_map(
        functools.partial(local, mesh.shape["ep"], mesh.shape["tp"]),
        mesh=mesh,
        in_specs=placed,
        out_specs=(P(("ep", "tp"), None), P(("ep", "tp"), None)),
        check_vma=False,
    )
```

time: 192 us -> 189 us (0.984); the launches traced: 189 us -> 188 us
  Pallas kernels: 173 us -> 185 us
  local copies, waits for them, and re-layouts: 8.01 us -> 2.47 us
  other arithmetic: 5.04 us -> 0 us
    pallas_call x1, Pallas kernels: 173 us -> 185 us  [local(): pl.pallas_call(functools.partial(body, n_ep, n_tp), out_shape=(jax.ShapeD...]
    unnamed x17 -> x4, local copies, waits for them, and re-layouts: 6.73 us -> 2.47 us
    reduce_sum x4 -> x0, other arithmetic: 2.73 us -> none  [the longest x1 1.44 us: route(): combine = jnp.sum(jnp.where(table, route_weights[:, :, None], 0.0), axis=1)]
where the time goes in v2:
time: 189 us; the launch traced here: 188 us
  Pallas kernels  185 us (98%)
  local copies, waits for them, and re-layouts  2.47 us (1%)
    pallas_call x1, Pallas kernels, local(): pl.pallas_call(functools.partial(body, n_ep, n_tp), out_shape=(jax.ShapeD...  185 us

profile of v2, /device:TPU:1, one launch (start us, length us, event | category | flops | bytes accessed | tf_op | source)
XLA Modules:
  0.0 187.9 jit_solution(14866721819675310260)
XLA Ops:
  0.6 184.7 %whole.1 = (bf16[64,2048]{1,0:T(8,128)(2,1)}, bf16[96,2048]{1,0:T(8,128)(2,1)}) custom-call(bf16[64,1024]{1,0:T(8,128)(2,1)} %bitcast.13, bf16[64,1024]{1,0:T(8,128)(2,1)} %bitcast.14, bf16[64,1024]{1,0:T(8,128)(2,1)} %bitcast.15, f32[8,128]{1,0:T(8,128)} %bitcast.17, bf16[2048,128]{1,0:T(8,128)(2,1)} %bitcast.10, bf16[2048,128]{1,0:T(8,128)(2,1)} %bitcast.11, ...), custom_call_target="tpu_custom_call" | custom-call | tf_op jit(solution)/shard_map/whole/pallas_call | solution.py:573
  185.4 0.0 copy-start
  185.4 1.7 copy.16
  187.1 0.0 copy-done
  187.1 0.7 copy.17
Async XLA Ops:
  185.4 1.7 copy-start

commit v3 on v2

--- a/solution.py
+++ b/solution.py
@@ -9,7 +9,7 @@
 from jax.sharding import PartitionSpec as P
 
 SLOT = 16
-TQ = 256
+SIDE = 4
 HEAD = 64
 MESH = pl.DeviceIdType.MESH
 
@@ -30,13 +30,13 @@
 
 
 def attend_block(q_ref, cq_ref, kv_ref, ck_ref, m_ref, l_ref, acc_ref, diagonal):
-    width = kv_ref.shape[0]
-    tile = min(TQ, q_ref.shape[0])
-    ck_row = gate_row(ck_ref[...])
-
-    def one_tile(i, carry):
-        rows = pl.ds(pl.multiple_of(i * tile, tile), tile)
-        kv = kv_ref[...]
+    tile = q_ref.shape[0] // 2
+    ck_all_row = gate_row(ck_ref[...])
+    for i in range(2):
+        rows = pl.ds(i * tile, tile)
+        width = (i + 1) * tile if diagonal else kv_ref.shape[0]
+        kv = kv_ref[:width, :]
+        ck_row = ck_all_row[:, :width]
         s = lax.dot_general(
             q_ref[rows, :], kv, (((1,), (1,)), ((), ())), preferred_element_type=jnp.float32
         )
@@ -63,9 +63,6 @@
             acc_ref[rows, :] = acc_ref[rows, :] * shrink + jnp.dot(
                 p.astype(jnp.bfloat16), kv, preferred_element_type=jnp.float32
             )
-        return carry
-
-    lax.fori_loop(0, q_ref.shape[0] // tile, one_tile, 0)
 
 
 N_BLOCKS = 4
@@ -95,7 +92,6 @@
     eo_ref,
     q_ref,
     cq_ref,
-    kv_ref,
     og_ref,
     comb_ref,
     kv_all,
@@ -112,7 +108,6 @@
     p_recv,
     res,
     ret,
-    osl,
     w_all,
     att_send,
     att_in,
@@ -178,8 +173,88 @@
             device_id={"tp": peer}, device_id_type=MESH,
         )
 
-    def kv_copy(slot, peer):
-        return ep_copy(kv_ref, kv_all.at[slot], s_kv.at[peer], r_kv.at[slot], peer)
+    y = lax.div(ep, SIDE)
+    x_at = lax.rem(ep, SIDE)
+    x_next = y * SIDE + lax.rem(x_at + 1, SIDE)
+    x_prev = y * SIDE + lax.rem(x_at + SIDE - 1, SIDE)
+    x_far = y * SIDE + lax.rem(x_at + 2, SIDE)
+    y_next = lax.rem(y + 1, SIDE)
+    y_prev = lax.rem(y + SIDE - 1, SIDE)
+    y_far = lax.rem(y + 2, SIDE)
+
+    class Spread:
+        def __init__(self, buf, send, recv):
+            self.buf, self.send, self.recv = buf, send, recv
+            self.half = buf.shape[1] // 2
+
+        def move(self, n, region, peer):
+            return ep_copy(region, region, self.send.at[n], self.recv.at[n], peer)
+
+        def part(self, slot, n):
+            return self.buf.at[slot, pl.ds(n * self.half, self.half)]
+
+        def rows(self, row, n, count):
+            return self.buf.at[pl.ds(row * SIDE + n, count)]
+
+        def sent(self, step):
+            if step == 1:
+                return (
+                    self.move(0, self.buf.at[ep], x_next),
+                    self.move(1, self.buf.at[ep], x_prev),
+                )
+            if step == 2:
+                return (
+                    self.move(2, self.part(x_prev, 0), x_next),
+                    self.move(3, self.part(x_next, 1), x_prev),
+                )
+            up, down = y_next * SIDE + x_at, y_prev * SIDE + x_at
+            if step == 3:
+                return (
+                    self.move(4, self.rows(y, 0, SIDE), up),
+                    self.move(5, self.rows(y, 0, SIDE), down),
+                )
+            return (
+                self.move(6, self.rows(y_prev, 0, SIDE // 2), up),
+                self.move(7, self.rows(y_next, SIDE // 2, SIDE // 2), down),
+            )
+
+        def come(self, step):
+            if step == 1:
+                return (
+                    self.move(0, self.buf.at[x_prev], x_next),
+                    self.move(1, self.buf.at[x_next], x_prev),
+                )
+            if step == 2:
+                return (
+                    self.move(2, self.part(x_far, 0), x_next),
+                    self.move(3, self.part(x_far, 1), x_prev),
+                )
+            up, down = y_next * SIDE + x_at, y_prev * SIDE + x_at
+            if step == 3:
+                return (
+                    self.move(4, self.rows(y_prev, 0, SIDE), up),
+                    self.move(5, self.rows(y_next, 0, SIDE), down),
+                )
+            return (
+                self.move(6, self.rows(y_far, 0, SIDE // 2), up),
+                self.move(7, self.rows(y_far, SIDE // 2, SIDE // 2), down),
+            )
+
+        def wait(self, step):
+            for copy in self.come(step):
+                copy.wait_recv()
+
+        def start(self, step):
+            for copy in self.sent(step):
+                copy.start()
+
+        def done(self):
+            for step in range(1, 5):
+                for copy in self.sent(step):
+                    copy.wait_send()
+
+    kv_spread = Spread(kv_all, s_kv, r_kv)
+    w_spread = Spread(w_all, s_w, r_w)
 
     def ck_copy(slot, peer):
         return ep_copy(ck_ref, ck_all.at[slot], s_ck.at[peer], r_ck.at[slot], peer)
@@ -192,14 +267,11 @@
             res.at[b, peer], ret.at[b, slot], s_res.at[b, peer], r_res.at[b, slot], peer
         )
 
-    def w_copy(slot, peer):
-        return ep_copy(osl, w_all.at[slot], s_w.at[peer], r_w.at[slot], peer)
-
     my_cols = pl.ds(pl.multiple_of(ep * col, col), col)
 
     def osl_copy(slot, pz):
         return tp_copy(
-            ow_ref.at[:, my_cols], osl.at[slot], s_osl.at[pz], r_osl.at[slot], 2 * pz + core
+            ow_ref.at[:, my_cols], w_all.at[ep, slot], s_osl.at[pz], r_osl.at[slot], 2 * pz + core
         )
 
     def att_copy(slot, pz):
@@ -295,7 +367,7 @@
             gu_first(direction, j).start()
     each(1, nz, lambda d: osl_copy(z, z_peer(d)).start())
 
-    kv_ref[...] = (
+    kv_all[ep] = (
         jnp.concatenate([kt_ref[...].astype(f32), vt_ref[...].astype(f32)], axis=0)
         .T.astype(bf16)
     )
@@ -336,23 +408,16 @@
         .reshape(n_ep, SLOT, width)
     )
 
-    attend_block(q_ref, cq_ref, kv_ref, ck_ref, m_ref, l_ref, att_acc, True)
-
-    def send_kv(d):
-        kv_copy(ep, ep + d).start()
-        ck_copy(ep, ep + d).start()
-
-    near = jnp.minimum(n_ep - ep, 4)
-    each(1, near, send_kv)
+    attend_block(q_ref, cq_ref, kv_all.at[ep], ck_ref, m_ref, l_ref, att_acc, True)
+
+    kv_spread.start(1)
+    each(1, n_ep - ep, lambda d: ck_copy(ep, ep + d).start())
     each(1, n_ep, lambda d: og_copy(ep, ep_peer(d)).start())
-    each(near, n_ep - ep, send_kv)
     x[0, ep] = og_ref[ep]
-    osl[z] = ow_ref[:, my_cols]
+    w_all[ep, z] = ow_ref[:, my_cols]
     dn[0] = wd_ref[...]
 
-    def attend_step(k):
-        j = ep - k
-        kv_copy(j, j).wait_recv()
+    def attend_step(j):
         ck_copy(j, j).wait_recv()
         attend_block(q_ref, cq_ref, kv_all.at[j], ck_all.at[j], m_ref, l_ref, att_acc, False)
 
@@ -364,64 +429,85 @@
             u = jnp.dot(rows, u_ref[...], preferred_element_type=f32)
             act[half, :, cols] = activate(g, u)
 
-    per_step = -(-(n_ep - 1) // (2 * hops - 1))
-
-    def hop_step(h, carry):
-        for j in range(2):
-            for direction in range(2):
-                @pl.when(h == 0)
-                def _():
-                    gu_first(direction, j).wait_recv()
-
-                @pl.when(h > 0)
-                def _():
-                    gu_next(direction, h, j).wait_recv()
-
-                @pl.when(h < hops - 1)
-                def _():
-                    gu_next(direction, h + 1, j).start()
-
-                if j == 0:
-                    @pl.when(h == hops - 1)
-                    def _():
-                        gu_last(direction).start()
-
-            if j == 1:
-                @pl.when(h == hops - 1)
-                def _():
-                    for i in range(3):
-                        start_down(i)
-
-                @pl.when(h == 0)
-                def _():
-                    each(1, n_ep, lambda d: og_copy(ep_peer(d), ep_peer(d)).wait_recv())
-                    x_copy().start()
-                    each(1, nz, lambda d: osl_copy(z_peer(d), z_peer(d)).wait_recv())
-                    each(1, n_ep, lambda d: w_copy(ep, ep_peer(d)).start())
-                    w_all[ep] = osl[...]
-
-            k0 = (2 * h + j) * per_step + 1
-            each(k0, jnp.minimum(k0 + per_step, ep + 1), attend_step)
-
-        @pl.when(h == 0)
-        def _():
-            x_copy().wait_recv()
-            expert_units(wg_ref, wu_ref, 0)
-
+    def units_of(h):
         for direction in range(2):
             expert_units(rg.at[direction, h], ru.at[direction, h], 1 + 2 * h + direction)
-        return carry
-
-    lax.fori_loop(0, hops, hop_step, 0)
-
-    for pz in range(nz):
-        rows = pl.ds(pz * 2 * t_dev, 2 * t_dev)
-        o = (att_acc[rows, :] / l_ref[rows, :])[:, HEAD:]
-        att_send[pz] = jnp.concatenate([o[:t_dev], o[t_dev:]], axis=1).astype(bf16)
-    for direction in range(2):
-        gu_last(direction).wait_recv()
+
+    def kv_step(step):
+        kv_spread.wait(step - 1)
+        kv_spread.start(step)
+
+    def w_step(step):
+        w_spread.wait(step - 1)
+        w_spread.start(step)
+
+    def first_w():
+        each(1, nz, lambda d: osl_copy(z_peer(d), z_peer(d)).wait_recv())
+        w_spread.start(1)
+
+    def swap_rows():
+        each(1, n_ep, lambda d: og_copy(ep_peer(d), ep_peer(d)).wait_recv())
+        x_copy().start()
+
+    def own_units():
+        x_copy().wait_recv()
+        expert_units(wg_ref, wu_ref, 0)
+
+    def send_attention():
+        for pz in range(nz):
+            rows = pl.ds(pz * 2 * t_dev, 2 * t_dev)
+            o = (att_acc[rows, :] / l_ref[rows, :])[:, HEAD:]
+            att_send[pz] = jnp.concatenate([o[:t_dev], o[t_dev:]], axis=1).astype(bf16)
+        att_in[z] = att_send[z]
+
+    def above(n):
+        return SIDE * jnp.maximum(y - n, 0)
+
+    def units_safe(h):
+        if h < hops:
+            units_of(h)
+
+    work_list = [
+        (0, lambda: kv_step(2)),
+        (0, first_w),
+        (1, lambda: kv_step(3)),
+        (1, swap_rows),
+        (1, lambda: each(SIDE * y, ep, attend_step)),
+        (1, lambda: w_step(2)),
+        (2, own_units),
+        (2, lambda: units_safe(0)),
+        (3, lambda: kv_step(4)),
+        (3, lambda: each(above(1), SIDE * y, attend_step)),
+        (4, lambda: w_step(3)),
+        (4, lambda: units_safe(1)),
+        (4, lambda: each(0, above(2), attend_step)),
+        (5, lambda: kv_spread.wait(4)),
+        (5, lambda: each(above(2), above(1), attend_step)),
+        (6, send_attention),
+        (6, lambda: w_step(4)),
+        (6, lambda: units_safe(2)),
+    ]
+    for n in range(firsts):
+        h, j = n // 2, n % 2
+        for direction in range(2):
+            if n == firsts - 1:
+                gu_last(direction).wait_recv()
+            elif h == 0:
+                gu_first(direction, j).wait_recv()
+            else:
+                gu_next(direction, h, j).wait_recv()
+            follow = n + 2
+            if follow < firsts - 1:
+                gu_next(direction, h + 1, j).start()
+            elif follow == firsts - 1:
+                gu_last(direction).start()
+        if n == firsts - 2:
+            for i in range(3):
+                start_down(i)
+        for at, work in work_list:
+            if min(at, firsts - 1) == n:
+                work()
     each(1, nz, lambda d: att_copy(z, z_peer(d)).start())
-    att_in[z] = att_send[z]
     expert_units(lg, lu, 1 + 2 * hops)
 
     def gather_heads():
@@ -433,7 +519,7 @@
         heads_ref[pl.ds(t_dev, t_dev), :] = jnp.concatenate(
             [t[:, HEAD:] for t in got], axis=1
         ).astype(bf16)
-        each(1, n_ep, lambda d: w_copy(ep_peer(d), ep_peer(d)).wait_recv())
+        w_spread.wait(4)
 
     def project(e):
         piece = w_all[e].reshape(nz * HEAD, col)
@@ -524,13 +610,9 @@
         for i in range(count):
             down_copy(direction, i).wait_send()
     each(1, n_ep, lambda d: og_copy(ep, ep_peer(d)).wait_send())
-    each(1, n_ep, lambda d: w_copy(ep, ep_peer(d)).wait_send())
-
-    def sent_kv(d):
-        kv_copy(ep, ep + d).wait_send()
-        ck_copy(ep, ep + d).wait_send()
-
-    each(1, n_ep - ep, sent_kv)
+    kv_spread.done()
+    w_spread.done()
+    each(1, n_ep - ep, lambda d: ck_copy(ep, ep + d).wait_send())
     x_copy().wait_send()
     mp_copy().wait_send()
     for b in range(N_BLOCKS):
@@ -581,7 +663,6 @@
         scratch_shapes=[
             vmem((block, 128), bf16),
             vmem((block, 1), f32),
-            vmem((block, 128), bf16),
             vmem((n_ep, SLOT, width), bf16),
             vmem((tokens, slots_all), f32),
             vmem((n_ep, block, 128), bf16),
@@ -598,7 +679,6 @@
             vmem((N_BLOCKS, slots_all, part), bf16),
             vmem((N_BLOCKS, n_ep, SLOT, part), bf16),
             vmem((N_BLOCKS, n_ep, SLOT, part), bf16),
-            vmem((nz, head, col), bf16),
             vmem((n_ep, nz, head, col), bf16),
             vmem((nz, t_dev, 128), bf16),
             vmem((nz, t_dev, 128), bf16),
@@ -610,7 +690,9 @@
             vmem((block, 128), f32),
             vmem((block, 128), f32),
         ]
-        + [dma((n_ep,))] * 8
+        + [dma((8,))] * 2
+        + [dma((n_ep,))] * 4
+        + [dma((8,))] * 2
         + [dma((nz,))] * 4
         + [dma((N_BLOCKS, n_ep))] * 2
         + [dma((2, items))] * 2

time: 189 us -> 158 us (0.84)
  Pallas kernels: 185 us -> 155 us
    pallas_call x1, Pallas kernels: 185 us -> 155 us  [local(): pl.pallas_call(functools.partial(body, n_ep, n_tp), out_shape=(jax.ShapeD...]
where the time goes in v3:
time: 158 us
  Pallas kernels  155 us (98%)
  local copies, waits for them, and re-layouts  2.47 us (2%)
    pallas_call x1, Pallas kernels, local(): pl.pallas_call(functools.partial(body, n_ep, n_tp), out_shape=(jax.ShapeD...  155 us

profile of v3, /device:TPU:1, one launch (start us, length us, event | category | flops | bytes accessed | tf_op | source)
XLA Modules:
  0.0 158.3 jit_solution(14719626276963994318)
XLA Ops:
  0.6 155.2 %whole.1 = (bf16[64,2048]{1,0:T(8,128)(2,1)}, bf16[96,2048]{1,0:T(8,128)(2,1)}) custom-call(bf16[64,1024]{1,0:T(8,128)(2,1)} %bitcast.13, bf16[64,1024]{1,0:T(8,128)(2,1)} %bitcast.14, bf16[64,1024]{1,0:T(8,128)(2,1)} %bitcast.15, f32[8,128]{1,0:T(8,128)} %bitcast.17, bf16[2048,128]{1,0:T(8,128)(2,1)} %bitcast.10, bf16[2048,128]{1,0:T(8,128)(2,1)} %bitcast.11, ...), custom_call_target="tpu_custom_call" | custom-call | tf_op jit(solution)/shard_map/whole/pallas_call | solution.py:655
  155.9 0.0 copy-start
  155.9 1.7 %copy.16 = bf16[64,2048]{1,0:T(8,128)(2,1)} copy(bf16[64,2048]{1,0:T(8,128)(2,1)} %get-tuple-element.4) | data formatting | bytes 524288
  157.6 0.0 copy-done
  157.6 0.7 copy.17
Async XLA Ops:
  155.9 1.7 %copy-start = (bf16[96,2048]{1,0:T(8,128)(2,1)S(1)}, bf16[96,2048]{1,0:T(8,128)(2,1)}, u32[]{:S(2)}) copy-start(bf16[96,2048]{1,0:T(8,128)(2,1)} %get-tuple-element.5) | copy-start | bytes 1179652

commit v4 on v3

--- a/solution.py
+++ b/solution.py
@@ -65,7 +65,8 @@
             )
 
 
-N_BLOCKS = 4
+SHARES = (5, 5, 4, 2)
+N_BLOCKS = len(SHARES)
 DOWN_ORDER = {
     3: ((0, 0), (1, 0), (2, 0), (0, 1), (1, 1), (0, 2), (2, 1), (0, 3), (1, 2), (3, 0),
         (1, 3), (2, 2), (3, 1), (2, 3), (3, 2), (3, 3)),
@@ -76,20 +77,27 @@
 def body(
     n_ep,
     n_tp,
-    qt_ref,
-    kt_ref,
-    vt_ref,
+    qt_in,
+    kt_in,
+    vt_in,
     ck_ref,
-    wg_ref,
-    wu_ref,
-    wd_ref,
-    ow_ref,
-    tok_ref,
+    wg_in,
+    wu_in,
+    wd_in,
+    ow_in,
+    tok_in,
     gain_ref,
     choice_ref,
     route_ref,
     mix_ref,
     eo_ref,
+    qt_ref,
+    kt_ref,
+    vt_ref,
+    wg_ref,
+    wu_ref,
+    ow_ref,
+    tok_ref,
     q_ref,
     cq_ref,
     og_ref,
@@ -136,6 +144,7 @@
     r_ring,
     s_pt,
     r_pt,
+    s_in,
 ):
     bf16, f32 = jnp.bfloat16, jnp.float32
     nz = n_tp // 2
@@ -147,12 +156,14 @@
     right = lax.rem(tp + 2, n_tp)
     left = lax.rem(tp + n_tp - 2, n_tp)
     partner = tp + 1 - 2 * core
-    units, width = wd_ref.shape
+    units, width = wd_in.shape
     block = q_ref.shape[0]
     tokens = tok_ref.shape[0]
     slots_all = n_ep * SLOT
     col = width // n_ep
-    part = width // N_BLOCKS
+    unit = width // 16
+    sizes = [n * unit for n in SHARES]
+    offsets = [sum(sizes[:b]) for b in range(N_BLOCKS)]
     t_dev = mp_send.shape[0]
 
     def ep_peer(d):
@@ -264,7 +275,9 @@
 
     def res_copy(b, slot, peer):
         return ep_copy(
-            res.at[b, peer], ret.at[b, slot], s_res.at[b, peer], r_res.at[b, slot], peer
+            res.at[b, peer, :, pl.ds(0, sizes[b])],
+            ret.at[b, slot, :, pl.ds(0, sizes[b])],
+            s_res.at[b, peer], r_res.at[b, slot], peer
         )
 
     my_cols = pl.ds(pl.multiple_of(ep * col, col), col)
@@ -289,10 +302,11 @@
         return pt_copy(mp_send, mp_recv, 1)
 
     def p_copy(b):
-        return pt_copy(p_send.at[b], p_recv.at[b], 2 + b)
+        cols = pl.ds(0, sizes[b])
+        return pt_copy(p_send.at[b, :, cols], p_recv.at[b, :, cols], 2 + b)
 
     peers = (right, left)
-    own = (wg_ref, wu_ref)
+    own = (wg_in, wu_in)
     slots = (rg, ru)
     last = (lg, lu)
     firsts = 2 * hops + 1
@@ -319,7 +333,7 @@
 
     def down_copy(direction, i):
         b, h = down_order[i]
-        cols = pl.ds(b * part, part)
+        cols = pl.ds(offsets[b], sizes[b])
         n = firsts + i
         rows = pl.ds(0, units)
         to = 1 + 2 * h + direction
@@ -327,7 +341,7 @@
             rows = pl.ds(direction * (units // 2), units // 2)
             to = 1 + 2 * hops
         if h == 0:
-            src = wd_ref.at[rows, cols]
+            src = dn.at[0, rows, cols]
         else:
             src = dn.at[1 + 2 * (h - 1) + direction, rows, cols]
         return tp_copy(
@@ -345,6 +359,24 @@
             return carry
 
         lax.fori_loop(start, stop, run, 0)
+
+    loads = [
+        pltpu.make_async_copy(src, dst, s_in.at[n])
+        for n, (src, dst) in enumerate(
+            (
+                (ow_in, ow_ref),
+                (kt_in, kt_ref),
+                (vt_in, vt_ref),
+                (qt_in, qt_ref),
+                (tok_in, tok_ref),
+                (wg_in, wg_ref),
+                (wu_in, wu_ref),
+                (wd_in, dn.at[0]),
+            )
+        )
+    ]
+    for load in loads:
+        load.start()
 
     barrier = pltpu.get_barrier_semaphore()
     each(
@@ -362,10 +394,14 @@
     pl.semaphore_signal(barrier, inc=1, device_id={"tp": partner}, device_id_type=MESH)
     pl.semaphore_wait(barrier, n_ep - 1 + nz - 1 + 1)
 
-    for j in range(2):
-        for direction in range(2):
-            gu_first(direction, j).start()
+    for direction in range(2):
+        gu_first(direction, 0).start()
+    loads[0].wait()
     each(1, nz, lambda d: osl_copy(z, z_peer(d)).start())
+    for direction in range(2):
+        gu_first(direction, 1).start()
+    for load in loads[1:]:
+        load.wait()
 
     kv_all[ep] = (
         jnp.concatenate([kt_ref[...].astype(f32), vt_ref[...].astype(f32)], axis=0)
@@ -415,7 +451,6 @@
     each(1, n_ep, lambda d: og_copy(ep, ep_peer(d)).start())
     x[0, ep] = og_ref[ep]
     w_all[ep, z] = ow_ref[:, my_cols]
-    dn[0] = wd_ref[...]
 
     def attend_step(j):
         ck_copy(j, j).wait_recv()
@@ -539,16 +574,19 @@
         mix_ref[...] = (mix_acc[mine, :] + mp_recv[...].astype(f32)).astype(bf16)
 
     def finish_units(b):
-        weights = dn[:, :, b * part : (b + 1) * part].reshape(nz * units, part)
-        p_send[b] = jnp.dot(act[1], weights, preferred_element_type=f32).astype(bf16)
+        size = sizes[b]
+        weights = dn[:, :, offsets[b] : offsets[b] + size].reshape(nz * units, size)
+        p_send[b, :, :size] = jnp.dot(act[1], weights, preferred_element_type=f32).astype(bf16)
         p_copy(b).start()
-        acc[b] = jnp.dot(act[0], weights, preferred_element_type=f32)
+        acc[b, :, :size] = jnp.dot(act[0], weights, preferred_element_type=f32)
 
     def send_home(b):
         p_copy(b).wait_recv()
-        res[b] = (acc[b] + p_recv[b].astype(f32)).astype(bf16).reshape(n_ep, SLOT, part)
+        size = sizes[b]
+        total = acc[b, :, :size] + p_recv[b, :, :size].astype(f32)
+        res[b, :, :, :size] = total.astype(bf16).reshape(n_ep, SLOT, size)
         each(1, n_ep, lambda d: res_copy(b, ep, ep_peer(d)).start())
-        ret[b, ep] = res[b, ep]
+        ret[b, ep, :, :size] = res[b, ep, :, :size]
 
     c0 = comb_ref[...]
     c_hi = c0.astype(bf16)
@@ -558,11 +596,12 @@
 
     def combine(b):
         each(1, n_ep, lambda d: res_copy(b, ep_peer(d), ep_peer(d)).wait_recv())
-        back = ret[b].reshape(slots_all, part)
+        size = sizes[b]
+        back = ret[b, :, :, :size].reshape(slots_all, size)
         total = jnp.dot(c_hi, back, preferred_element_type=f32)
         total += jnp.dot(c_mid, back, preferred_element_type=f32)
         total += jnp.dot(c_lo, back, preferred_element_type=f32)
-        eo_ref[:, b * part : (b + 1) * part] = total.astype(bf16)
+        eo_ref[:, offsets[b] : offsets[b] + size] = total.astype(bf16)
 
     count = len(down_order)
     issued = 3
@@ -646,7 +685,7 @@
     hops = nz // 2 - 1
     t_dev = block // n_tp
     col = width // n_ep
-    part = width // N_BLOCKS
+    part = max(SHARES) * width // 16
     slots_all = n_ep * SLOT
     items = 2 * hops + 1 + len(DOWN_ORDER[hops])
     bf16, f32 = jnp.bfloat16, jnp.float32
@@ -658,9 +697,18 @@
             jax.ShapeDtypeStruct((t_dev, width), bf16),
             jax.ShapeDtypeStruct((tokens, width), bf16),
         ),
-        in_specs=[pl.BlockSpec(memory_space=vmem)] * 12,
+        in_specs=[
+            pl.BlockSpec(memory_space=vmem if n in (3, 9, 10, 11) else pl.ANY) for n in range(12)
+        ],
         out_specs=(pl.BlockSpec(memory_space=vmem),) * 2,
         scratch_shapes=[
+            vmem((head, block), bf16),
+            vmem((head, block), bf16),
+            vmem((head, block), bf16),
+            vmem((width, units), bf16),
+            vmem((width, units), bf16),
+            vmem((head, width), bf16),
+            vmem((tokens, width), bf16),
             vmem((block, 128), bf16),
             vmem((block, 1), f32),
             vmem((n_ep, SLOT, width), bf16),
@@ -696,9 +744,10 @@
         + [dma((nz,))] * 4
         + [dma((N_BLOCKS, n_ep))] * 2
         + [dma((2, items))] * 2
-        + [dma((2 + N_BLOCKS,))] * 2,
+        + [dma((2 + N_BLOCKS,))] * 2
+        + [dma((8,))],
         compiler_params=pltpu.CompilerParams(
-            collective_id=0, has_side_effects=True, vmem_limit_bytes=60 * 2**20
+            collective_id=0, has_side_effects=True, vmem_limit_bytes=63 * 2**20
         ),
         name="whole",
     )(

time: 158 us -> 159 us (level)
  no operation moved by 1% of the time
where the time goes in v4:
time: 159 us
  Pallas kernels  156 us (98%)
  local copies, waits for them, and re-layouts  2.47 us (2%)
    pallas_call x1, Pallas kernels, local(): pl.pallas_call(functools.partial(body, n_ep, n_tp), out_shape=(jax.ShapeD...  156 us

profile of v4, /device:TPU:1, one launch (start us, length us, event | category | flops | bytes accessed | tf_op | source)
XLA Modules:
  0.0 158.9 jit_solution(10594382269494733390)
XLA Ops:
  0.6 155.8 %whole.1 = (bf16[64,2048]{1,0:T(8,128)(2,1)}, bf16[96,2048]{1,0:T(8,128)(2,1)}) custom-call(bf16[64,1024]{1,0:T(8,128)(2,1)} %bitcast.13, bf16[64,1024]{1,0:T(8,128)(2,1)} %bitcast.14, bf16[64,1024]{1,0:T(8,128)(2,1)} %bitcast.15, f32[8,128]{1,0:T(8,128)} %bitcast.17, bf16[2048,128]{1,0:T(8,128)(2,1)} %bitcast.10, bf16[2048,128]{1,0:T(8,128)(2,1)} %bitcast.11, ...), custom_call_target="tpu_custom_call" | custom-call | tf_op jit(solution)/shard_map/whole/pallas_call | solution.py:694
  156.4 0.0 copy-start
  156.4 1.7 %copy.16 = bf16[64,2048]{1,0:T(8,128)(2,1)} copy(bf16[64,2048]{1,0:T(8,128)(2,1)} %get-tuple-element.4) | data formatting | bytes 524288
  158.1 0.0 copy-done
  158.1 0.7 copy.17
Async XLA Ops:
  156.4 1.7 %copy-start = (bf16[96,2048]{1,0:T(8,128)(2,1)S(1)}, bf16[96,2048]{1,0:T(8,128)(2,1)}, u32[]{:S(2)}) copy-start(bf16[96,2048]{1,0:T(8,128)(2,1)} %get-tuple-element.5) | copy-start | bytes 1179652

commit v5 on v4

--- a/solution.py
+++ b/solution.py
@@ -68,8 +68,8 @@
 SHARES = (5, 5, 4, 2)
 N_BLOCKS = len(SHARES)
 DOWN_ORDER = {
-    3: ((0, 0), (1, 0), (2, 0), (0, 1), (1, 1), (0, 2), (2, 1), (0, 3), (1, 2), (3, 0),
-        (1, 3), (2, 2), (3, 1), (2, 3), (3, 2), (3, 3)),
+    3: ((0, 0), (1, 0), (2, 0), (1, 1), (0, 1), (1, 2), (0, 2), (1, 3), (2, 1), (0, 3),
+        (3, 0), (2, 2), (3, 1), (2, 3), (3, 2), (3, 3)),
     1: ((0, 0), (1, 0), (2, 0), (0, 1), (1, 1), (3, 0), (2, 1), (3, 1)),
 }
 
@@ -306,7 +306,7 @@
         return pt_copy(p_send.at[b, :, cols], p_recv.at[b, :, cols], 2 + b)
 
     peers = (right, left)
-    own = (wg_in, wu_in)
+    own = (wg_ref, wu_ref)
     slots = (rg, ru)
     last = (lg, lu)
     firsts = 2 * hops + 1
@@ -364,13 +364,13 @@
         pltpu.make_async_copy(src, dst, s_in.at[n])
         for n, (src, dst) in enumerate(
             (
+                (wg_in, wg_ref),
+                (wu_in, wu_ref),
                 (ow_in, ow_ref),
                 (kt_in, kt_ref),
                 (vt_in, vt_ref),
                 (qt_in, qt_ref),
                 (tok_in, tok_ref),
-                (wg_in, wg_ref),
-                (wu_in, wu_ref),
                 (wd_in, dn.at[0]),
             )
         )
@@ -394,13 +394,14 @@
     pl.semaphore_signal(barrier, inc=1, device_id={"tp": partner}, device_id_type=MESH)
     pl.semaphore_wait(barrier, n_ep - 1 + nz - 1 + 1)
 
+    for load in loads[:3]:
+        load.wait()
     for direction in range(2):
         gu_first(direction, 0).start()
-    loads[0].wait()
     each(1, nz, lambda d: osl_copy(z, z_peer(d)).start())
     for direction in range(2):
         gu_first(direction, 1).start()
-    for load in loads[1:]:
+    for load in loads[3:]:
         load.wait()
 
     kv_all[ep] = (
@@ -619,22 +620,22 @@
         for direction in range(2):
             down_copy(direction, i).wait_recv()
         arrived.append(down_order[i])
-        while issued < min(count, i + 3):
+        while issued < count:
             b, h = down_order[issued]
             if h > 0 and (b, h - 1) not in arrived:
                 break
             start_down(issued)
             issued += 1
-        for b in pending:
+        for due, b in [p for p in pending if p[0] <= i]:
             send_home(b)
-        pending = []
+        pending = [p for p in pending if p[0] > i]
         b, h = down_order[i]
         if h == hops:
             finish_units(b)
-            pending.append(b)
+            pending.append((i + 2 if i + 4 < count else i + 1, b))
         elif i >= mixer_at and mixer_work:
             mixer_work.pop(0)()
-    for b in pending:
+    for due, b in pending:
         send_home(b)
     for work in mixer_work:
         work()

time: 159 us -> 158 us (level)
  Pallas kernels: 156 us -> 154 us
where the time goes in v5:
time: 158 us; the launch traced here: 157 us
  Pallas kernels  154 us (97%)
  local copies, waits for them, and re-layouts  2.47 us (2%)
    pallas_call x1, Pallas kernels, local(): pl.pallas_call(functools.partial(body, n_ep, n_tp), out_shape=(jax.ShapeD...  154 us

profile of v5, /device:TPU:1, one launch (start us, length us, event | category | flops | bytes accessed | tf_op | source)
XLA Modules:
  0.0 157.4 jit_solution(13619959575869057329)
XLA Ops:
  0.6 154.3 %whole.1 = (bf16[64,2048]{1,0:T(8,128)(2,1)}, bf16[96,2048]{1,0:T(8,128)(2,1)}) custom-call(bf16[64,1024]{1,0:T(8,128)(2,1)} %bitcast.13, bf16[64,1024]{1,0:T(8,128)(2,1)} %bitcast.14, bf16[64,1024]{1,0:T(8,128)(2,1)} %bitcast.15, f32[8,128]{1,0:T(8,128)} %bitcast.17, bf16[2048,128]{1,0:T(8,128)(2,1)} %bitcast.10, bf16[2048,128]{1,0:T(8,128)(2,1)} %bitcast.11, ...), custom_call_target="tpu_custom_call" | custom-call | tf_op jit(solution)/shard_map/whole/pallas_call | solution.py:695
  155.0 0.0 copy-start
  155.0 1.7 %copy.16 = bf16[64,2048]{1,0:T(8,128)(2,1)} copy(bf16[64,2048]{1,0:T(8,128)(2,1)} %get-tuple-element.4) | data formatting | bytes 524288
  156.7 0.0 copy-done
  156.7 0.7 copy.17
Async XLA Ops:
  155.0 1.7 %copy-start = (bf16[96,2048]{1,0:T(8,128)(2,1)S(1)}, bf16[96,2048]{1,0:T(8,128)(2,1)}, u32[]{:S(2)}) copy-start(bf16[96,2048]{1,0:T(8,128)(2,1)} %get-tuple-element.5) | copy-start | bytes 1179652

commit v6 on v5

--- a/solution.py
+++ b/solution.py
@@ -543,7 +543,6 @@
         for at, work in work_list:
             if min(at, firsts - 1) == n:
                 work()
-    each(1, nz, lambda d: att_copy(z, z_peer(d)).start())
     expert_units(lg, lu, 1 + 2 * hops)
 
     def gather_heads():
@@ -615,7 +614,7 @@
             functools.partial(each, q * quarter, min((q + 1) * quarter, n_ep), project)
         )
     mixer_work += [send_mix, take_mix]
-    mixer_at = min(4, count - 8) if count > 8 else 0
+    mixer_at = count
     for i in range(count):
         for direction in range(2):
             down_copy(direction, i).wait_recv()
@@ -626,6 +625,8 @@
                 break
             start_down(issued)
             issued += 1
+        if i == count - 4:
+            each(1, nz, lambda d: att_copy(z, z_peer(d)).start())
         for due, b in [p for p in pending if p[0] <= i]:
             send_home(b)
         pending = [p for p in pending if p[0] > i]
@@ -637,7 +638,7 @@
             mixer_work.pop(0)()
     for due, b in pending:
         send_home(b)
-    for work in mixer_work:
+    for work in mixer_work[:-1]:
         work()
 
     each(1, nz, lambda d: osl_copy(z, z_peer(d)).wait_send())
@@ -654,11 +655,13 @@
     w_spread.done()
     each(1, n_ep - ep, lambda d: ck_copy(ep, ep + d).wait_send())
     x_copy().wait_send()
-    mp_copy().wait_send()
     for b in range(N_BLOCKS):
         p_copy(b).wait_send()
-    for b in range(N_BLOCKS):
+    for b in range(N_BLOCKS - 1):
         combine(b)
+    take_mix()
+    combine(N_BLOCKS - 1)
+    mp_copy().wait_send()
     for b in range(N_BLOCKS):
         each(1, n_ep, lambda d: res_copy(b, ep, ep_peer(d)).wait_send())
 

time: 158 us -> 155 us (0.981)
  Pallas kernels: 154 us -> 152 us
    pallas_call x1, Pallas kernels: 154 us -> 152 us  [local(): pl.pallas_call(functools.partial(body, n_ep, n_tp), out_shape=(jax.ShapeD...]
where the time goes in v6:
time: 155 us
  Pallas kernels  152 us (98%)
  local copies, waits for them, and re-layouts  2.47 us (2%)
    pallas_call x1, Pallas kernels, local(): pl.pallas_call(functools.partial(body, n_ep, n_tp), out_shape=(jax.ShapeD...  152 us

profile of v6, /device:TPU:1, one launch (start us, length us, event | category | flops | bytes accessed | tf_op | source)
XLA Modules:
  0.0 155.3 jit_solution(14731644599721686630)
XLA Ops:
  0.6 152.2 %whole.1 = (bf16[64,2048]{1,0:T(8,128)(2,1)}, bf16[96,2048]{1,0:T(8,128)(2,1)}) custom-call(bf16[64,1024]{1,0:T(8,128)(2,1)} %bitcast.13, bf16[64,1024]{1,0:T(8,128)(2,1)} %bitcast.14, bf16[64,1024]{1,0:T(8,128)(2,1)} %bitcast.15, f32[8,128]{1,0:T(8,128)} %bitcast.17, bf16[2048,128]{1,0:T(8,128)(2,1)} %bitcast.10, bf16[2048,128]{1,0:T(8,128)(2,1)} %bitcast.11, ...), custom_call_target="tpu_custom_call" | custom-call | tf_op jit(solution)/shard_map/whole/pallas_call | solution.py:698
  152.8 0.0 copy-start
  152.9 1.7 %copy.16 = bf16[64,2048]{1,0:T(8,128)(2,1)} copy(bf16[64,2048]{1,0:T(8,128)(2,1)} %get-tuple-element.4) | data formatting | bytes 524288
  154.6 0.0 copy-done
  154.6 0.7 copy.17
Async XLA Ops:
  152.8 1.7 %copy-start = (bf16[96,2048]{1,0:T(8,128)(2,1)S(1)}, bf16[96,2048]{1,0:T(8,128)(2,1)}, u32[]{:S(2)}) copy-start(bf16[96,2048]{1,0:T(8,128)(2,1)} %get-tuple-element.5) | copy-start | bytes 1179652
